TPU v7x, 32 devices: a whole 2x2x4 slice. The times are simulated.
32 devices in a mesh: ep: 32 (over z, y, x, core).
Axes of the slice: x: 2, y: 2, z: 4, core: 2. Of those that a mesh axis runs over, the one named last changes fastest.
Arguments:
- tokens: bfloat16 [1024, 3072], P('ep'), may hold values from -6 to 6
- norm_gain: float32 [3072], replicated, may hold values from 0.1 to 1.9
- expert_ids: int32 [1024, 4], P('ep'), may hold values from 0 to 31, as said below
- expert_scores: float32 [1024, 4], P('ep'), may hold values from -100 to 180
- group_prob: float32 [1024], P('ep'), may hold values from 0.25 to 1
- gate_weight: bfloat16 [32, 3072, 384], P('ep'), may hold values from -0.109375 to 0.109375
- up_weight: bfloat16 [32, 3072, 384], P('ep'), may hold values from -0.109375 to 0.109375
- down_weight: bfloat16 [32, 384, 3072], P('ep'), may hold values from -0.3125 to 0.3125
Outputs:
- combined: bfloat16 [1024, 3072], P('ep')
Inputs may be any that keep to these rules, and one draw needn't show every extreme that they name: `expert_ids`: the 4 ids of a row are different and lie in one group of 8 consecutive experts. Among the rows of one device no expert is named by more than 16 rows, and in every draw some expert is named by exactly 16 rows of one device.
All inputs are finite; a program needn't handle non-finite values.
Results may differ from a plain program's by a relative error of at most 0.0085.
Values may be sent and summed in bfloat16 or wider, within the bound.
A program may use at most 128 MiB of HBM per device.

v0:
```python
import functools

import jax
import jax.numpy as jnp
from jax import lax
from jax.experimental import pallas as pl
from jax.experimental.pallas import tpu as pltpu
from jax.sharding import PartitionSpec as P

GROUPS = 4
TOP_K = 4
LANES = 128
MESH = pl.DeviceIdType.MESH


eps_norm = 1e-05


def layer_norm(tokens, norm_gain):
    values = tokens.astype(jnp.float32)
    average = jnp.mean(values, axis=1, keepdims=True)
    centred = values - average
    variance = jnp.mean(centred * centred, axis=1, keepdims=True)
    return (centred * lax.rsqrt(variance + eps_norm) * norm_gain[None, :]).astype(jnp.bfloat16)


def mixing_weights(expert_scores, group_prob):
    shifted = expert_scores - jnp.max(expert_scores, axis=1, keepdims=True)
    exp_scores = jnp.exp(shifted)
    return exp_scores / jnp.sum(exp_scores, axis=1, keepdims=True) * group_prob[:, None]


def expert_rows(flat_rows, gate_matrix, up_matrix, down_matrix):
    gate_act = jnp.dot(flat_rows, gate_matrix, preferred_element_type=jnp.float32)
    up_act = jnp.dot(flat_rows, up_matrix, preferred_element_type=jnp.float32)
    hidden = (jax.nn.silu(gate_act) * up_act).astype(jnp.bfloat16)
    return jnp.dot(hidden, down_matrix, preferred_element_type=jnp.float32).astype(jnp.bfloat16)


def local(
    tokens, norm_gain, expert_ids, expert_scores, group_prob, gate_weight, up_weight, down_weight
):
    normed = layer_norm(tokens, norm_gain)
    weights_tok = mixing_weights(expert_scores, group_prob)
    tok_count = tokens.shape[0]
    model_width = tokens.shape[1]
    expert_count = lax.axis_size("ep")
    group_size = expert_count // GROUPS
    capacity = (tok_count * TOP_K + group_size - 1) // group_size
    expert_iota = jnp.arange(expert_count, dtype=jnp.int32)
    slot_iota = jnp.arange(capacity, dtype=jnp.int32)
    matches = expert_ids[:, :, None] == expert_iota[None, None, :]
    route_weight = jnp.sum(jnp.where(matches, weights_tok[:, :, None], 0.0), axis=1)
    gate_matrix = gate_weight[0]
    up_matrix = up_weight[0]
    down_matrix = down_weight[0]
    chosen = jnp.sum(matches.astype(jnp.int32), axis=1)
    order_rank = jnp.cumsum(chosen, axis=0) - chosen
    slot_map = (chosen.T[:, None, :] == 1) & (order_rank.T[:, None, :] == slot_iota[None, :, None])
    outgoing = jnp.einsum(
        "emt,td->emd", slot_map.astype(jnp.bfloat16), normed, preferred_element_type=jnp.float32
    ).astype(jnp.bfloat16)
    received = lax.all_to_all(outgoing, "ep", split_axis=0, concat_axis=0, tiled=True)
    flat_rows = received.reshape(-1, model_width)
    results = expert_rows(flat_rows, gate_matrix, up_matrix, down_matrix).reshape(received.shape)
    returned_rows = lax.all_to_all(results, "ep", split_axis=0, concat_axis=0, tiled=True)
    slot_scale = jnp.where(slot_map, route_weight.T[:, None, :], 0.0)
    mixture = jnp.einsum(
        "emt,emd->td",
        slot_scale,
        returned_rows.astype(jnp.float32),
        precision=lax.Precision.HIGHEST,
    )
    return mixture.astype(jnp.bfloat16)

def ring_kernel(
    zs, tok_ref, gain_ref, ids_ref, score_ref, prob_ref, gate_hbm, up_hbm, down_hbm, out_ref,
    x0, x1, p0, p1, rd0, rd1, rb0, rb1, ra0, ra1, rz0, rz1, wg, wu, wd, w_sem,
    gather_recv, gather_pair_recv, gather_z, gather_x, gather_y, gather_pair,
    pair_recv, pair_send, far_recv, far_send, near_recv, near_send, line_recv, line_send,
):
    xs, ps, rds, rbs, ras, rzs = (x0, x1), (p0, p1), (rd0, rd1), (rb0, rb1), (ra0, ra1), (rz0, rz1)
    me = lax.axis_index("ep")
    core = lax.rem(me, 2)
    x = lax.rem(lax.div(me, 2), 2)
    y = lax.rem(lax.div(me, 4), 2)
    z = lax.div(me, 8)

    def device(zz, yy, xx, cc):
        return ((zz * 2 + yy) * 2 + xx) * 2 + cc

    partner = device(z, y, x, 1 - core)
    x_side = device(z, y, 1 - x, core)
    y_side = device(z, 1 - y, x, core)
    z_side = (device(z - 1, y, x, core), device(z + 1, y, x, core))
    has = (z > 0, z < zs - 1)
    chunks = [yy * 2 + xx for yy in (y, 1 - y) for xx in (x, 1 - x)]

    def base(rel, cc):
        return (chunks[rel] * 2 + cc) * zs

    copies = [
        pltpu.make_async_copy(src.at[0], dst, w_sem.at[i])
        for i, (src, dst) in enumerate(((gate_hbm, wg), (up_hbm, wu), (down_hbm, wd)))
    ]
    for copy in copies:
        copy.start()

    barrier = pltpu.get_barrier_semaphore()
    for other in (partner, x_side, y_side):
        pl.semaphore_signal(barrier, inc=1, device_id=(other,), device_id_type=MESH)
    for d in (0, 1):
        @pl.when(has[d])
        def _():
            pl.semaphore_signal(barrier, inc=1, device_id=(z_side[d],), device_id_type=MESH)

    model_width = tok_ref.shape[1]
    half = x0.shape[2]
    values = tok_ref[...].astype(jnp.float32)
    average = jnp.sum(values, axis=1, keepdims=True) * (1.0 / model_width)
    centred = values - average
    variance = jnp.sum(centred * centred, axis=1, keepdims=True) * (1.0 / model_width)
    normed = (centred * lax.rsqrt(variance + eps_norm) * gain_ref[...]).astype(jnp.bfloat16)
    count = tok_ref.shape[0]
    score = [score_ref[k : k + 1, :] for k in range(TOP_K)]
    top = functools.reduce(jnp.maximum, score)
    exps = [jnp.exp(s - top) for s in score]
    total = functools.reduce(jnp.add, exps)
    row = lax.broadcasted_iota(jnp.int32, (LANES, count), 0)
    tags = jnp.zeros((LANES, count), jnp.float32)
    for k in range(TOP_K):
        weight = exps[k] / total * prob_ref[...]
        high = weight.astype(jnp.bfloat16).astype(jnp.float32)
        tags = jnp.where(row == k, ids_ref[k : k + 1, :].astype(jnp.float32), tags)
        tags = jnp.where(row == TOP_K + k, high, tags)
        tags = jnp.where(row == 2 * TOP_K + k, weight - high, tags)
    square = (count, count)
    same = lax.broadcasted_iota(jnp.int32, square, 0) == lax.broadcasted_iota(jnp.int32, square, 1)
    meta = lax.dot_general(
        same.astype(jnp.float32).astype(jnp.bfloat16), tags.astype(jnp.bfloat16),
        (((1,), (1,)), ((), ())), preferred_element_type=jnp.float32,
    )
    own = base(0, core) + z
    x0[own] = normed[:, :half]
    x1[own, :, : model_width - half] = normed[:, half:]
    x1[own, :, model_width - half :] = meta.astype(jnp.bfloat16)

    inside = jnp.logical_and(has[0], has[1])

    @pl.when(inside)
    def _():
        pl.semaphore_wait(barrier, 5)

    @pl.when(jnp.logical_not(inside))
    def _():
        pl.semaphore_wait(barrier, 4)

    pending = []

    def send(src, dst, send_sem, recv_sem, target, conds=()):
        array, index = send_sem
        pltpu.make_async_remote_copy(
            src_ref=src(), dst_ref=dst(), send_sem=array.at[index], recv_sem=recv_sem,
            device_id=(target,), device_id_type=MESH,
        ).start()

        def finish():
            sem = array.at[index]
            pltpu.make_async_remote_copy(
                src_ref=src(), dst_ref=dst(), send_sem=sem, recv_sem=sem,
                device_id=(target,), device_id_type=MESH,
            ).wait_send()

        pending.append((conds, finish))

    def landed(dst, recv_sem):
        pltpu.make_async_remote_copy(
            src_ref=dst, dst_ref=dst, send_sem=recv_sem, recv_sem=recv_sem,
            device_id=(partner,), device_id_type=MESH,
        ).wait_recv()

    def at_distance(s, body):
        if s == 0:
            body(z, (), None)
            return
        for d, q, ok in ((1, z - s, z - s >= 0), (0, z + s, z + s < zs)):
            @pl.when(ok)
            def _():
                body(q, (ok,), d)

    def spread(q, conds, came):
        for h in (0, 1):
            block = functools.partial(lambda h: xs[h].at[base(0, core) + q], h)
            if came is not None:
                landed(block(), gather_recv.at[h, 0, q])
            for d in (0, 1):
                if came is None or came == d:
                    @pl.when(has[d])
                    def _():
                        send(block, block, (gather_z, (h, d, q)), gather_recv.at[h, 0, q],
                             z_side[d], conds + (has[d],))
            send(block, block, (gather_x, (h, 0, q)), gather_recv.at[h, 1, q], x_side, conds)
            send(block, block, (gather_y, (h, 0, q)), gather_recv.at[h, 2, q], y_side, conds)

    def forward(q, conds, _):
        block = lambda: x0.at[base(1, core) + q]
        landed(block(), gather_recv.at[0, 1, q])
        send(block, block, (gather_y, (0, 1, q)), gather_recv.at[0, 3, q], y_side, conds)
        other = lambda: x1.at[base(2, core) + q]
        landed(other(), gather_recv.at[1, 2, q])
        send(other, other, (gather_x, (1, 1, q)), gather_recv.at[1, 3, q], x_side, conds)

    def all_landed(h, rel):
        for q in range(zs):
            landed(xs[h].at[base(rel, core) + q], gather_recv.at[h, rel, q])

    def pair_gather(rel):
        for h in (0, 1):
            blocks = functools.partial(lambda h: xs[h].at[pl.ds(base(rel, core), zs)], h)
            send(blocks, blocks, (gather_pair, (h, rel)), gather_pair_recv.at[h, rel], partner)

    def compute(rel):
        for h in (0, 1):
            landed(xs[h].at[pl.ds(base(rel, 1 - core), zs)], gather_pair_recv.at[h, rel])
        slots = pl.ds(chunks[rel] * 2 * zs, 2 * zs)
        rows = 2 * zs * tok_ref.shape[0]
        left = x0[slots].reshape(rows, half)
        right = x1[slots, :, : model_width - half].reshape(rows, model_width - half)
        tags = x1[slots, :, model_width - half :].reshape(rows, LANES).astype(jnp.float32)
        expert = me.astype(jnp.float32)
        scale = jnp.zeros((rows, 1), jnp.float32)
        for k in range(TOP_K):
            value = tags[:, TOP_K + k : TOP_K + k + 1] + tags[:, 2 * TOP_K + k : 2 * TOP_K + k + 1]
            scale += jnp.where(tags[:, k : k + 1] == expert, value, 0.0)

        def project(w):
            return jnp.dot(left, w[:half, :], preferred_element_type=jnp.float32) + jnp.dot(
                right, w[half:, :], preferred_element_type=jnp.float32
            )

        gate_act = project(wg)
        up_act = project(wu)
        hidden = (jax.nn.silu(gate_act) * up_act).astype(jnp.bfloat16)
        step = half // 3 if half % (3 * LANES) == 0 else half
        for h in (0, 1):
            width = ps[h].shape[2]
            for at in range(0, width, step):
                part = jnp.dot(hidden, wd[:, h * half + at : h * half + at + step],
                               preferred_element_type=jnp.float32)
                part = (part.astype(jnp.bfloat16).astype(jnp.float32) * scale).astype(jnp.bfloat16)
                ps[h][slots, :, at : at + step] = part.reshape(2 * zs, tok_ref.shape[0], step)

    def pair_reduce(rel):
        for h in (0, 1):
            part = functools.partial(lambda h: ps[h].at[pl.ds(base(rel, 1 - core), zs)], h)
            room = functools.partial(lambda h: rds[h].at[rel], h)
            send(part, room, (pair_send, (h, rel)), pair_recv.at[h, rel], partner)

    def pair_add(rel):
        for h in (0, 1):
            landed(rds[h].at[rel], pair_recv.at[h, rel])
            slots = pl.ds(base(rel, core), zs)
            ps[h][slots] = ps[h][slots] + rds[h][rel]

    far_side = (y_side, x_side)
    near_side = (x_side, y_side)

    def far(h, rel, kind):
        def body(q, conds, _):
            send(lambda: ps[h].at[base(rel, core) + q], lambda: rbs[h].at[kind, q],
                 (far_send, (h, kind, q)), far_recv.at[h, kind, q], far_side[h], conds)
        return body

    def near(q, conds, _):
        for h in (0, 1):
            landed(rbs[h].at[1, q], far_recv.at[h, 1, q])
            slot = base(1 + h, core) + q
            ps[h][slot] = ps[h][slot] + rbs[h][1, q]
            part = functools.partial(lambda h: ps[h].at[base(1 + h, core) + q], h)
            room = functools.partial(lambda h: ras[h].at[q], h)
            send(part, room, (near_send, (h, q)), near_recv.at[h, q],
                 near_side[h], conds)

    def line(q, conds, d):
        for h in (0, 1):
            landed(rbs[h].at[0, q], far_recv.at[h, 0, q])
            landed(ras[h].at[q], near_recv.at[h, q])
            slot = base(0, core) + q
            held = ps[h][slot].astype(jnp.float32) + rbs[h][0, q].astype(jnp.float32)
            ps[h][slot] = (held + ras[h][q].astype(jnp.float32)).astype(jnp.bfloat16)
            if d is None:
                for side in (0, 1):
                    @pl.when(has[side])
                    def _():
                        landed(rzs[h].at[side, q], line_recv.at[h, side, q])
                        ps[h][slot] = ps[h][slot] + rzs[h][side, q]
                width = ps[h].shape[2]
                out_ref[:, h * half : h * half + width] = ps[h][slot]
            else:
                @pl.when(has[d])
                def _():
                    landed(rzs[h].at[d, q], line_recv.at[h, d, q])
                    ps[h][slot] = ps[h][slot] + rzs[h][d, q]
                part = functools.partial(lambda h: ps[h].at[base(0, core) + q], h)
                room = functools.partial(lambda h: rzs[h].at[d, q], h)
                send(part, room, (line_send, (h, d, q)),
                     line_recv.at[h, d, q], z_side[1 - d], conds)

    def far_first(body):
        for s in range(zs - 1, -1, -1):
            at_distance(s, body)

    at_distance(0, spread)
    for s in range(1, zs):
        at_distance(s, spread)
        at_distance(s - 1, forward)
    pair_gather(0)
    for copy in copies:
        copy.wait()
    compute(0)
    pair_reduce(0)
    at_distance(zs - 1, forward)
    all_landed(1, 1)
    pair_gather(1)
    all_landed(0, 2)
    pair_gather(2)
    compute(1)
    pair_reduce(1)
    pair_add(1)
    far_first(far(1, 1, 0))
    compute(2)
    pair_reduce(2)
    pair_add(0)
    pair_add(2)
    far_first(far(0, 2, 0))
    for h in (0, 1):
        all_landed(h, 3)
    pair_gather(3)
    compute(3)
    pair_reduce(3)
    pair_add(3)
    far_first(far(0, 3, 1))
    far_first(far(1, 3, 1))
    at_distance(zs - 1, near)
    for s in range(zs - 2, -1, -1):
        at_distance(s, near)
        at_distance(s + 1, line)
    at_distance(0, line)

    for conds, finish in pending:
        if conds:
            pl.when(functools.reduce(jnp.logical_and, conds))(finish)
        else:
            finish()


def ring_local(
    zs, tokens, norm_gain, expert_ids, expert_scores, group_prob, gate_weight, up_weight, down_weight
):
    count, width = tokens.shape
    hidden = gate_weight.shape[2]
    slots = zs * 8
    half = width // 2
    kind = jnp.bfloat16
    vmem = pl.BlockSpec(memory_space=pltpu.VMEM)
    hbm = pl.BlockSpec(memory_space=pl.ANY)
    dma = pltpu.SemaphoreType.DMA
    widths = (half, width - half)
    each = lambda *lead: [pltpu.VMEM(lead + (count, w), kind) for w in widths]
    scratch = [
        pltpu.VMEM((slots, count, half), kind),
        pltpu.VMEM((slots, count, width - half + LANES), kind),
        *each(slots), *each(4, zs), *each(2, zs), *each(zs), *each(2, zs),
        pltpu.VMEM((width, hidden), kind), pltpu.VMEM((width, hidden), kind),
        pltpu.VMEM((hidden, width), kind), dma((3,)),
        dma((2, 4, zs)), dma((2, 4)), dma((2, 2, zs)), dma((2, 2, zs)), dma((2, 2, zs)), dma((2, 4)),
        dma((2, 4)), dma((2, 4)), dma((2, 2, zs)), dma((2, 2, zs)),
        dma((2, zs)), dma((2, zs)), dma((2, 2, zs)), dma((2, 2, zs)),
    ]
    return pl.pallas_call(
        functools.partial(ring_kernel, zs),
        out_shape=jax.ShapeDtypeStruct((count, width), kind),
        in_specs=[vmem] * 5 + [hbm] * 3,
        out_specs=vmem,
        scratch_shapes=scratch,
        compiler_params=pltpu.CompilerParams(
            collective_id=0, has_side_effects=True, vmem_limit_bytes=60 * 1024 * 1024
        ),
    )(
        tokens, norm_gain[None, :], expert_ids.T, expert_scores.T, group_prob[None, :], gate_weight, up_weight, down_weight,
    )


def solution(mesh):
    in_specs = (
        P("ep", None),
        P(),
        P("ep", None),
        P("ep", None),
        P("ep"),
        P("ep", None, None),
        P("ep", None, None),
        P("ep", None, None),
    )
    out_specs = P("ep", None)
    devices = mesh.shape["ep"]
    body = functools.partial(ring_local, GROUPS) if devices == GROUPS * 8 else local
    return jax.shard_map(body, mesh=mesh, in_specs=in_specs, out_specs=out_specs, check_vma=False)
```

profile of v0, /device:TPU:0, one launch (start us, length us, event | category | flops | bytes accessed | tf_op | source)
XLA Modules:
  0.0 79.5 jit_solution(17802242280412603456)
XLA Ops:
  0.0 77.9 %shard_map.82 = bf16[32,3072]{1,0:T(8,128)(2,1)} custom-call(bf16[32,3072]{1,0:T(8,128)(2,1)} %tok_ref.1, f32[1,3072]{1,0:T(1,128)} %bitcast.4, s32[4,32]{1,0:T(4,128)} %bitcast.5, f32[4,32]{1,0:T(4,128)} %bitcast.6, f32[1,32]{1,0:T(1,128)} %bitcast.7, bf16[1,3072,384]{2,1,0:T(8,128)(2,1)} %gate_hbm.1, bf16[1,3072,384]{2,1,0:T(8,128)(2,1)} %up_hbm.1, ...), custom_call_target="tpu_custom_call" | custom-call | tf_op jit(solution)/shard_map/pallas_call | solution.py:380
  77.9 1.6 %copy.10 = bf16[32,3072]{1,0:T(8,128)(2,1)} copy(bf16[32,3072]{1,0:T(8,128)(2,1)} %shard_map.82) | data formatting | bytes 393216
where the time goes:
time: 79.9 us; the launch traced here: 79.5 us
  Pallas kernels  77.9 us (97%)
  local copies, waits for them, and re-layouts  1.62 us (2%)
    pallas_call x1, Pallas kernels, ring_local(): pl.pallas_call(functools.partial(ring_kernel, zs), out_shape=jax.ShapeDty...  77.9 us
    unnamed x1, local copies, waits for them, and re-layouts  1.62 us

commit v1 on v0

v1 whole, which is shorter than its diff:
```python
import functools

import jax
import jax.numpy as jnp
from jax import lax
from jax.experimental import pallas as pl
from jax.experimental.pallas import tpu as pltpu
from jax.sharding import PartitionSpec as P

GROUPS = 4
TOP_K = 4
LANES = 128
MESH = pl.DeviceIdType.MESH


eps_norm = 1e-05


def layer_norm(tokens, norm_gain):
    values = tokens.astype(jnp.float32)
    average = jnp.mean(values, axis=1, keepdims=True)
    centred = values - average
    variance = jnp.mean(centred * centred, axis=1, keepdims=True)
    return (centred * lax.rsqrt(variance + eps_norm) * norm_gain[None, :]).astype(jnp.bfloat16)


def mixing_weights(expert_scores, group_prob):
    shifted = expert_scores - jnp.max(expert_scores, axis=1, keepdims=True)
    exp_scores = jnp.exp(shifted)
    return exp_scores / jnp.sum(exp_scores, axis=1, keepdims=True) * group_prob[:, None]


def expert_rows(flat_rows, gate_matrix, up_matrix, down_matrix):
    gate_act = jnp.dot(flat_rows, gate_matrix, preferred_element_type=jnp.float32)
    up_act = jnp.dot(flat_rows, up_matrix, preferred_element_type=jnp.float32)
    hidden = (jax.nn.silu(gate_act) * up_act).astype(jnp.bfloat16)
    return jnp.dot(hidden, down_matrix, preferred_element_type=jnp.float32).astype(jnp.bfloat16)


def local(
    tokens, norm_gain, expert_ids, expert_scores, group_prob, gate_weight, up_weight, down_weight
):
    normed = layer_norm(tokens, norm_gain)
    weights_tok = mixing_weights(expert_scores, group_prob)
    tok_count = tokens.shape[0]
    model_width = tokens.shape[1]
    expert_count = lax.axis_size("ep")
    group_size = expert_count // GROUPS
    capacity = (tok_count * TOP_K + group_size - 1) // group_size
    expert_iota = jnp.arange(expert_count, dtype=jnp.int32)
    slot_iota = jnp.arange(capacity, dtype=jnp.int32)
    matches = expert_ids[:, :, None] == expert_iota[None, None, :]
    route_weight = jnp.sum(jnp.where(matches, weights_tok[:, :, None], 0.0), axis=1)
    gate_matrix = gate_weight[0]
    up_matrix = up_weight[0]
    down_matrix = down_weight[0]
    chosen = jnp.sum(matches.astype(jnp.int32), axis=1)
    order_rank = jnp.cumsum(chosen, axis=0) - chosen
    slot_map = (chosen.T[:, None, :] == 1) & (order_rank.T[:, None, :] == slot_iota[None, :, None])
    outgoing = jnp.einsum(
        "emt,td->emd", slot_map.astype(jnp.bfloat16), normed, preferred_element_type=jnp.float32
    ).astype(jnp.bfloat16)
    received = lax.all_to_all(outgoing, "ep", split_axis=0, concat_axis=0, tiled=True)
    flat_rows = received.reshape(-1, model_width)
    results = expert_rows(flat_rows, gate_matrix, up_matrix, down_matrix).reshape(received.shape)
    returned_rows = lax.all_to_all(results, "ep", split_axis=0, concat_axis=0, tiled=True)
    slot_scale = jnp.where(slot_map, route_weight.T[:, None, :], 0.0)
    mixture = jnp.einsum(
        "emt,emd->td",
        slot_scale,
        returned_rows.astype(jnp.float32),
        precision=lax.Precision.HIGHEST,
    )
    return mixture.astype(jnp.bfloat16)

CHUNKS = 4


def plan():
    order = []

    def at(time, *step):
        order.append((time, len(order), step))

    for k in range(CHUNKS):
        base = 6.3 * k
        at(max(base - 4.0, 0.1 * k), "own", k)
        at(base + 2.5, "first", k)
        for i in range(1, 4):
            at(base + 2.5 + 2.3 * i, "line", k, i)
        for i in range(4):
            at(base + 4.9 + 2.3 * i, "last", k, i)
        ready = base + 14.0
        at(ready, "hidden", k)
        at(ready + 1.5, "down", k)
        at(ready + 4.0, "back", k)
        for i in range(3):
            at(ready + 7.5 + 2.3 * i, "sum", k, i)
        at(ready + 14.5, "home", k)
        at(ready + 17.0, "final", k)
        at(ready + 8.0, "drain_out", k)
        at(ready + 20.0, "drain_back", k)
    return [step for _, _, step in sorted(order)]


def ring_kernel(
    zs, tok_ref, gain_ref, ids_ref, score_ref, prob_ref, gate_hbm, up_hbm, down_hbm, out_ref,
    xg, stage, part, pair_in, last_in, line_in, first_in, fin_in, hid, scales, wgu, wd, w_sem,
    stage_send, stage_recv, gather_recv, own_send, first_send, line_send, last_send,
    mate_send, mate_recv, pair_send, pair_recv, back_send, back_recv, sum_send, sum_recv,
    home_send, home_recv, fin_send, fin_recv,
):
    me = lax.axis_index("ep")
    core = lax.rem(me, 2)
    x = lax.rem(lax.div(me, 2), 2)
    y = lax.rem(lax.div(me, 4), 2)
    z = lax.div(me, 8)
    other = 1 - core

    def device(zz, yy, xx, cc):
        return ((zz * 2 + yy) * 2 + xx) * 2 + cc

    partner = device(z, y, x, other)
    first_dev = device(z, y + core * (1 - 2 * y), x + other * (1 - 2 * x), core)
    last_dev = device(z, y + other * (1 - 2 * y), x + core * (1 - 2 * x), core)
    has = (z > 0, z < zs - 1)

    def column(fr, lr):
        dx = other * fr + core * lr
        dy = core * fr + other * lr
        xx = x + dx * (1 - 2 * x)
        yy = y + dy * (1 - 2 * y)
        return (xx * 2 + yy) * zs

    cols = [[column(fr, lr) for lr in (0, 1)] for fr in (0, 1)]
    near = [sorted(range(zs), key=lambda q, zz=zz: (abs(q - zz), -q if zz < zs // 2 else q))
            for zz in range(zs)]
    planes = []
    for i in range(zs):
        q = jnp.int32(near[0][i])
        for zz in range(1, zs):
            q = jnp.where(z == zz, near[zz][i], q)
        planes.append(q)
    below = [q < z for q in planes]
    away = [jnp.where(b, z + 1, z - 1) for b in below]
    away_ok = [jnp.logical_and(a >= 0, a < zs) for a in away]
    toward = [jnp.where(b, z - 1, z + 1) for b in below]
    side_of = [jnp.where(b, 1, 0) for b in below]

    model_width = tok_ref.shape[1]
    half = model_width // 2
    count = tok_ref.shape[0]
    rows = stage.shape[1]
    blocks = 4 * zs

    copies = [
        pltpu.make_async_copy(gate_hbm.at[0], wgu.at[:, : wgu.shape[1] // 2], w_sem.at[0]),
        pltpu.make_async_copy(up_hbm.at[0], wgu.at[:, wgu.shape[1] // 2 :], w_sem.at[1]),
        pltpu.make_async_copy(down_hbm.at[0, :, :half], wd.at[0], w_sem.at[2]),
        pltpu.make_async_copy(down_hbm.at[0, :, half:], wd.at[1], w_sem.at[3]),
    ]
    for copy in copies:
        copy.start()

    barrier = pltpu.get_barrier_semaphore()
    for peer in (partner, first_dev, last_dev):
        pl.semaphore_signal(barrier, inc=1, device_id=(peer,), device_id_type=MESH)
    for d in (0, 1):
        @pl.when(has[d])
        def _():
            pl.semaphore_signal(
                barrier, inc=1, device_id=(device(z - 1 + 2 * d, y, x, core),), device_id_type=MESH
            )

    def remote(src, dst, send_sem, recv_sem, target):
        return pltpu.make_async_remote_copy(
            src_ref=src, dst_ref=dst, send_sem=send_sem, recv_sem=recv_sem,
            device_id=(target,), device_id_type=MESH,
        )

    def landed(ref, sem):
        remote(ref, ref, sem, sem, partner).wait_recv()

    def sent(ref, sem):
        remote(ref, ref, sem, sem, partner).wait_send()

    def wide(k):
        return half + LANES if k == 0 else half

    def block(h, k, slot):
        return xg.at[h, k, slot, :, pl.ds(0, wide(k))]

    def span(h, k, n):
        return xg.at[h, k, pl.ds(0, n), :, pl.ds(0, wide(k))]

    own_slot = cols[0][0] + z

    values = tok_ref[...].astype(jnp.float32)
    average = jnp.sum(values, axis=1, keepdims=True) * (1.0 / model_width)
    centred = values - average
    variance = jnp.sum(centred * centred, axis=1, keepdims=True) * (1.0 / model_width)
    normed = (centred * lax.rsqrt(variance + eps_norm) * gain_ref[...]).astype(jnp.bfloat16)
    for c in (0, 1):
        @pl.when(core == c)
        def _():
            for j in range(CHUNKS // 2):
                piece = normed[j * rows : (j + 1) * rows]
                mine = piece[:, :half] if c == 0 else piece[:, half:]
                theirs = piece[:, half:] if c == 0 else piece[:, :half]
                xg[c, 2 * j + c, own_slot, :, :half] = mine
                stage[j] = theirs
    score = [score_ref[k : k + 1, :] for k in range(TOP_K)]
    top = functools.reduce(jnp.maximum, score)
    exps = [jnp.exp(s - top) for s in score]
    total = functools.reduce(jnp.add, exps)
    row = lax.broadcasted_iota(jnp.int32, (rows, count), 0)
    tags = jnp.zeros((rows, count), jnp.float32)
    for k in range(TOP_K):
        weight = exps[k] / total * prob_ref[...]
        high = weight.astype(jnp.bfloat16).astype(jnp.float32)
        tags = jnp.where(row == k, ids_ref[k : k + 1, :].astype(jnp.float32), tags)
        tags = jnp.where(row == TOP_K + k, high, tags)
        tags = jnp.where(row == 2 * TOP_K + k, weight - high, tags)
    tags = jnp.concatenate([tags, jnp.zeros((rows, LANES - count), jnp.float32)], axis=1)
    xg[core, 0, own_slot, :, half:] = tags.astype(jnp.bfloat16)

    inside = jnp.logical_and(has[0], has[1])

    @pl.when(inside)
    def _():
        pl.semaphore_wait(barrier, 5)

    @pl.when(jnp.logical_not(inside))
    def _():
        pl.semaphore_wait(barrier, 4)

    for j in range(CHUNKS // 2):
        k = 2 * j + core
        remote(stage.at[j], xg.at[core * 0 + other, k, own_slot, :, pl.ds(0, half)],
               stage_send.at[j], stage_recv.at[k], partner).start()

    def spread(k, slot, fr, i):
        ref = block(core, k, slot)
        sem = gather_recv.at[k, slot]
        if i == 0:
            for d in (0, 1):
                @pl.when(has[d])
                def _():
                    remote(ref, ref, own_send.at[k, d], sem, device(z - 1 + 2 * d, y, x, core)).start()
        else:
            @pl.when(away_ok[i])
            def _():
                remote(ref, ref, line_send.at[k, i], sem, device(away[i], y, x, core)).start()
        remote(ref, ref, last_send.at[k], sem, last_dev).start()
        remote(ref, ref, mate_send.at[k], mate_recv.at[k], partner).start()

    def own(k):
        @pl.when(core != k % 2)
        def _():
            landed(xg.at[core, k, own_slot, :, pl.ds(0, half)], stage_recv.at[k])
        ref = block(core, k, own_slot)
        remote(ref, ref, first_send.at[k], gather_recv.at[k, own_slot], first_dev).start()
        spread(k, own_slot, 0, 0)

    def first(k):
        slot = cols[1][0] + z
        landed(block(core, k, slot), gather_recv.at[k, slot])
        spread(k, slot, 1, 0)

    def line(k, i):
        for fr in (0, 1):
            slot = cols[fr][0] + planes[i]
            landed(block(core, k, slot), gather_recv.at[k, slot])
            spread(k, slot, fr, i)

    def last(k, i):
        for fr in (0, 1):
            slot = cols[fr][1] + planes[i]
            ref = block(core, k, slot)
            landed(ref, gather_recv.at[k, slot])
            remote(ref, ref, mate_send.at[k], mate_recv.at[k], partner).start()

    def hidden(k):
        landed(span(other, k, blocks), mate_recv.at[k])
        if k == 0:
            for copy in copies:
                copy.wait()
            expert = me.astype(jnp.float32)
            for h in (0, 1):
                tags = xg[h, 0, :, :, half:].astype(jnp.float32)
                scale = jnp.zeros((blocks, LANES), jnp.float32)
                for n in range(TOP_K):
                    value = tags[:, TOP_K + n, :] + tags[:, 2 * TOP_K + n, :]
                    scale += jnp.where(tags[:, n, :] == expert, value, 0.0)
                scales[h] = scale
        shape = (blocks, rows, LANES)
        pick = lax.broadcasted_iota(jnp.int32, shape, 2) == (
            lax.broadcasted_iota(jnp.int32, shape, 1) + rows * (k // 2))
        scale = jnp.sum(jnp.where(pick, scales[k % 2][:, None, :], 0.0), axis=2, keepdims=True)
        scale = scale.reshape(blocks * rows, 1)
        left = xg[0, k, :, :, :half].reshape(blocks * rows, half)
        right = xg[1, k, :, :, :half].reshape(blocks * rows, half)
        acts = jnp.dot(left, wgu[:half, :], preferred_element_type=jnp.float32) + jnp.dot(
            right, wgu[half:, :], preferred_element_type=jnp.float32
        )
        inner = hid.shape[1]
        hid[...] = (jax.nn.silu(acts[:, :inner]) * acts[:, inner:] * scale).astype(jnp.bfloat16)

    def down(k):
        step = half // 3 if half % (3 * LANES) == 0 else half
        for h in (other, core):
            for at in range(0, half, step):
                out = jnp.dot(hid[...], wd[h, :, at : at + step], preferred_element_type=jnp.float32)
                part[h, k, :, :, at : at + step] = out.astype(jnp.bfloat16).reshape(blocks, rows, step)
            if h is other:
                remote(part.at[other, k], pair_in.at[k], pair_send.at[k], pair_recv.at[k], partner).start()

    def back(k):
        landed(pair_in.at[k], pair_recv.at[k])
        for i in range(zs - 1, -1, -1):
            for fr in (0, 1):
                slot = cols[fr][1] + planes[i]
                part[core, k, slot] = part[core, k, slot] + pair_in[k, slot]
                remote(part.at[core, k, slot], last_in.at[k, fr, planes[i]], back_send.at[k],
                       back_recv.at[k, fr, planes[i]], last_dev).start()

    def gathered(k, fr, q):
        slot = cols[fr][0] + q
        landed(last_in.at[k, fr, q], back_recv.at[k, fr, q])
        held = part[core, k, slot].astype(jnp.float32) + pair_in[k, slot].astype(jnp.float32)
        part[core, k, slot] = (held + last_in[k, fr, q].astype(jnp.float32)).astype(jnp.bfloat16)
        return slot

    def line_sum(k, j):
        i = zs - 1 - j
        q = planes[i]
        for fr in (0, 1):
            slot = gathered(k, fr, q)

            @pl.when(away_ok[i])
            def _():
                landed(line_in.at[k, side_of[i], fr, q], sum_recv.at[k, side_of[i], fr, q])
                part[core, k, slot] = part[core, k, slot] + line_in[k, side_of[i], fr, q]

            remote(part.at[core, k, slot], line_in.at[k, side_of[i], fr, q], sum_send.at[k],
                   sum_recv.at[k, side_of[i], fr, q], device(toward[i], y, x, core)).start()

    def home(k):
        for fr in (1, 0):
            slot = gathered(k, fr, z)
            for d in (0, 1):
                @pl.when(has[d])
                def _():
                    landed(line_in.at[k, d, fr, z], sum_recv.at[k, d, fr, z])
                    part[core, k, slot] = part[core, k, slot] + line_in[k, d, fr, z]
            if fr == 1:
                remote(part.at[core, k, slot], first_in.at[k], home_send.at[k], home_recv.at[k],
                       first_dev).start()

    def final(k):
        landed(first_in.at[k], home_recv.at[k])
        total = part[core, k, own_slot] + first_in[k]
        j = k // 2

        @pl.when(core == k % 2)
        def _():
            out_ref[j * rows : (j + 1) * rows, pl.ds(pl.multiple_of(core * half, LANES), half)] = total

        @pl.when(core != k % 2)
        def _():
            part[core, k, own_slot] = total
            remote(part.at[core, k, own_slot], fin_in.at[j], fin_send.at[j], fin_recv.at[j],
                   partner).start()

    def drain_out(k):
        @pl.when(core == k % 2)
        def _():
            sent(stage.at[k // 2], stage_send.at[k // 2])
        sent(block(core, k, own_slot), first_send.at[k])
        for d in (0, 1):
            @pl.when(has[d])
            def _():
                sent(span(core, k, 2), own_send.at[k, d])
        for i in range(1, zs):
            @pl.when(away_ok[i])
            def _():
                sent(span(core, k, 2), line_send.at[k, i])
        sent(span(core, k, 2 * zs), last_send.at[k])
        sent(span(core, k, blocks), mate_send.at[k])

    def drain_back(k):
        sent(part.at[other, k], pair_send.at[k])
        sent(part.at[core, k, pl.ds(0, 2 * zs)], back_send.at[k])
        sent(part.at[core, k, pl.ds(0, 2 * (zs - 1))], sum_send.at[k])
        sent(part.at[core, k, 0], home_send.at[k])

    steps = dict(own=own, first=first, line=line, last=last, hidden=hidden, down=down, back=back,
                 sum=line_sum, home=home, final=final, drain_out=drain_out, drain_back=drain_back)
    for name, *rest in plan():
        steps[name](*rest)

    for j in range(CHUNKS // 2):
        landed(fin_in.at[j], fin_recv.at[j])
        out_ref[j * rows : (j + 1) * rows, pl.ds(pl.multiple_of(other * half, LANES), half)] = fin_in[j]
    for j in range(CHUNKS // 2):
        sent(fin_in.at[j], fin_send.at[j])


def ring_local(
    zs, tokens, norm_gain, expert_ids, expert_scores, group_prob, gate_weight, up_weight, down_weight
):
    count, width = tokens.shape
    inner = gate_weight.shape[2]
    half = width // 2
    rows = 2 * count // CHUNKS
    blocks = 4 * zs
    kind = jnp.bfloat16
    vmem = pl.BlockSpec(memory_space=pltpu.VMEM)
    hbm = pl.BlockSpec(memory_space=pl.ANY)
    dma = pltpu.SemaphoreType.DMA
    c = CHUNKS
    scratch = [
        pltpu.VMEM((2, c, blocks, rows, half + LANES), kind),
        pltpu.VMEM((c // 2, rows, half), kind),
        pltpu.VMEM((2, c, blocks, rows, half), kind),
        pltpu.VMEM((c, blocks, rows, half), kind),
        pltpu.VMEM((c, 2, zs, rows, half), kind),
        pltpu.VMEM((c, 2, 2, zs, rows, half), kind),
        pltpu.VMEM((c, rows, half), kind),
        pltpu.VMEM((c // 2, rows, half), kind),
        pltpu.VMEM((blocks * rows, inner), kind),
        pltpu.VMEM((2, blocks, LANES), jnp.float32),
        pltpu.VMEM((width, 2 * inner), kind),
        pltpu.VMEM((2, inner, half), kind),
        dma((4,)),
        dma((c // 2,)), dma((c,)), dma((c, blocks)), dma((c, 2)), dma((c,)), dma((c, zs)), dma((c,)),
        dma((c,)), dma((c,)), dma((c,)), dma((c,)), dma((c,)), dma((c, 2, zs)),
        dma((c,)), dma((c, 2, 2, zs)),
        dma((c,)), dma((c,)), dma((c // 2,)), dma((c // 2,)),
    ]
    return pl.pallas_call(
        functools.partial(ring_kernel, zs),
        out_shape=jax.ShapeDtypeStruct((count, width), kind),
        in_specs=[vmem] * 5 + [hbm] * 3,
        out_specs=vmem,
        scratch_shapes=scratch,
        compiler_params=pltpu.CompilerParams(
            collective_id=0, has_side_effects=True, vmem_limit_bytes=60 * 1024 * 1024
        ),
    )(
        tokens, norm_gain[None, :], expert_ids.T, expert_scores.T, group_prob[None, :], gate_weight, up_weight, down_weight,
    )


def solution(mesh):
    in_specs = (
        P("ep", None),
        P(),
        P("ep", None),
        P("ep", None),
        P("ep"),
        P("ep", None, None),
        P("ep", None, None),
        P("ep", None, None),
    )
    out_specs = P("ep", None)
    devices = mesh.shape["ep"]
    body = functools.partial(ring_local, GROUPS) if devices == GROUPS * 8 else local
    return jax.shard_map(body, mesh=mesh, in_specs=in_specs, out_specs=out_specs, check_vma=False)
```

time: 79.9 us -> 96.7 us (1.21)
  Pallas kernels: 77.9 us -> 94.1 us
    pallas_call x1, Pallas kernels: 77.9 us -> 94.1 us  [ring_local(): pl.pallas_call(functools.partial(ring_kernel, zs), out_shape=jax.ShapeDty...]
where the time goes in v1:
time: 96.7 us; the launch traced here: 95.7 us
  Pallas kernels  94.1 us (97%)
  local copies, waits for them, and re-layouts  1.62 us (2%)
    pallas_call x1, Pallas kernels, ring_local(): pl.pallas_call(functools.partial(ring_kernel, zs), out_shape=jax.ShapeDty...  94.1 us

profile of v1, /device:TPU:0, one launch (start us, length us, event | category | flops | bytes accessed | tf_op | source)
XLA Modules:
  0.0 95.7 jit_solution(2384362919076009288)
XLA Ops:
  0.0 94.1 %shard_map.82 = bf16[32,3072]{1,0:T(8,128)(2,1)} custom-call(bf16[32,3072]{1,0:T(8,128)(2,1)} %tok_ref.1, f32[1,3072]{1,0:T(1,128)} %bitcast.4, s32[4,32]{1,0:T(4,128)} %bitcast.5, f32[4,32]{1,0:T(4,128)} %bitcast.6, f32[1,32]{1,0:T(1,128)} %bitcast.7, bf16[1,3072,384]{2,1,0:T(8,128)(2,1)} %gate_hbm.1, bf16[1,3072,384]{2,1,0:T(8,128)(2,1)} %up_hbm.1, ...), custom_call_target="tpu_custom_call" | custom-call | tf_op jit(solution)/shard_map/pallas_call | solution.py:441
  94.1 1.6 %copy.10 = bf16[32,3072]{1,0:T(8,128)(2,1)} copy(bf16[32,3072]{1,0:T(8,128)(2,1)} %shard_map.82) | data formatting | bytes 393216

commit v2 on v1

--- a/solution.py
+++ b/solution.py
@@ -76,31 +76,30 @@
 CHUNKS = 4
 
 
-def plan():
-    order = []
-
-    def at(time, *step):
-        order.append((time, len(order), step))
-
-    for k in range(CHUNKS):
-        base = 6.3 * k
-        at(max(base - 4.0, 0.1 * k), "own", k)
-        at(base + 2.5, "first", k)
-        for i in range(1, 4):
-            at(base + 2.5 + 2.3 * i, "line", k, i)
-        for i in range(4):
-            at(base + 4.9 + 2.3 * i, "last", k, i)
-        ready = base + 14.0
-        at(ready, "hidden", k)
-        at(ready + 1.5, "down", k)
-        at(ready + 4.0, "back", k)
-        for i in range(3):
-            at(ready + 7.5 + 2.3 * i, "sum", k, i)
-        at(ready + 14.5, "home", k)
-        at(ready + 17.0, "final", k)
-        at(ready + 8.0, "drain_out", k)
-        at(ready + 20.0, "drain_back", k)
-    return [step for _, _, step in sorted(order)]
+ORDER = (
+    ("own", 2), ("own", 0), ("own", 1), ("first", 2), ("own", 3), ("first", 0), ("first", 1),
+    ("line", 1, 1, 0), ("line", 0, 1, 0), ("first", 3), ("line", 0, 2, 0), ("line", 1, 1, 1),
+    ("line", 1, 2, 1), ("last", 0, 2, 0), ("line", 0, 1, 1), ("line", 0, 3, 0), ("last", 1, 1, 0),
+    ("line", 0, 2, 1), ("last", 0, 0, 0), ("last", 0, 1, 0), ("line", 2, 1, 0), ("last", 0, 0, 1),
+    ("line", 0, 3, 1), ("line", 1, 2, 0), ("line", 1, 3, 1), ("last", 0, 2, 1), ("last", 1, 1, 1),
+    ("last", 1, 0, 0), ("last", 0, 1, 1), ("last", 1, 2, 1), ("last", 0, 3, 0), ("line", 2, 1, 1),
+    ("last", 2, 0, 0), ("line", 2, 2, 1), ("last", 1, 0, 1), ("last", 3, 0, 0), ("last", 0, 3, 1),
+    ("line", 1, 3, 0), ("line", 3, 2, 0), ("line", 2, 2, 0), ("line", 3, 1, 0), ("last", 1, 3, 1),
+    ("hidden", 0), ("line", 2, 3, 1), ("last", 1, 3, 0), ("line", 3, 1, 1), ("last", 1, 2, 0),
+    ("last", 2, 2, 1), ("down", 0), ("last", 2, 1, 1), ("last", 2, 1, 0), ("line", 2, 3, 0),
+    ("line", 3, 2, 1), ("hidden", 1), ("last", 2, 0, 1), ("last", 2, 3, 1), ("back", 0), ("down", 1),
+    ("line", 3, 3, 1), ("last", 2, 2, 0), ("last", 2, 3, 0), ("line", 3, 3, 0), ("last", 3, 0, 1),
+    ("sum", 0, 0, 1), ("sum", 0, 0, 0), ("back", 1), ("last", 3, 2, 1), ("last", 3, 1, 1), ("hidden", 2),
+    ("sum", 0, 1, 0), ("last", 3, 2, 0), ("sum", 0, 2, 1), ("sum", 0, 1, 1), ("last", 3, 3, 1),
+    ("last", 3, 3, 0), ("last", 3, 1, 0), ("down", 2), ("sum", 1, 0, 1), ("sum", 1, 0, 0), ("hidden", 3),
+    ("back", 2), ("sum", 1, 1, 1), ("sum", 0, 2, 0), ("down", 3), ("sum", 1, 2, 1), ("back", 3),
+    ("sum", 1, 2, 0), ("sum", 1, 1, 0), ("sum", 2, 0, 1), ("sum", 2, 0, 0), ("sum", 3, 0, 1),
+    ("sum", 3, 0, 0), ("sum", 2, 1, 1), ("sum", 3, 1, 1), ("sum", 2, 1, 0), ("sum", 3, 2, 1), ("home", 0, 1),
+    ("home", 1, 1), ("sum", 3, 1, 0), ("sum", 2, 2, 1), ("sum", 3, 2, 0), ("drain_out", 0), ("drain_out", 1),
+    ("drain_out", 2), ("drain_out", 3), ("home", 3, 1), ("sum", 2, 2, 0), ("home", 1, 0), ("final", 1),
+    ("home", 0, 0), ("home", 2, 1), ("home", 3, 0), ("final", 0), ("drain_back", 0), ("drain_back", 1),
+    ("drain_back", 2), ("final", 3), ("home", 2, 0), ("final", 2), ("drain_back", 3),
+)
 
 
 def ring_kernel(
@@ -267,18 +266,16 @@
         landed(block(core, k, slot), gather_recv.at[k, slot])
         spread(k, slot, 1, 0)
 
-    def line(k, i):
-        for fr in (0, 1):
-            slot = cols[fr][0] + planes[i]
-            landed(block(core, k, slot), gather_recv.at[k, slot])
-            spread(k, slot, fr, i)
-
-    def last(k, i):
-        for fr in (0, 1):
-            slot = cols[fr][1] + planes[i]
-            ref = block(core, k, slot)
-            landed(ref, gather_recv.at[k, slot])
-            remote(ref, ref, mate_send.at[k], mate_recv.at[k], partner).start()
+    def line(k, i, fr):
+        slot = cols[fr][0] + planes[i]
+        landed(block(core, k, slot), gather_recv.at[k, slot])
+        spread(k, slot, fr, i)
+
+    def last(k, i, fr):
+        slot = cols[fr][1] + planes[i]
+        ref = block(core, k, slot)
+        landed(ref, gather_recv.at[k, slot])
+        remote(ref, ref, mate_send.at[k], mate_recv.at[k], partner).start()
 
     def hidden(k):
         landed(span(other, k, blocks), mate_recv.at[k])
@@ -331,31 +328,29 @@
         part[core, k, slot] = (held + last_in[k, fr, q].astype(jnp.float32)).astype(jnp.bfloat16)
         return slot
 
-    def line_sum(k, j):
+    def line_sum(k, j, fr):
         i = zs - 1 - j
         q = planes[i]
-        for fr in (0, 1):
-            slot = gathered(k, fr, q)
-
-            @pl.when(away_ok[i])
+        slot = gathered(k, fr, q)
+
+        @pl.when(away_ok[i])
+        def _():
+            landed(line_in.at[k, side_of[i], fr, q], sum_recv.at[k, side_of[i], fr, q])
+            part[core, k, slot] = part[core, k, slot] + line_in[k, side_of[i], fr, q]
+
+        remote(part.at[core, k, slot], line_in.at[k, side_of[i], fr, q], sum_send.at[k],
+               sum_recv.at[k, side_of[i], fr, q], device(toward[i], y, x, core)).start()
+
+    def home(k, fr):
+        slot = gathered(k, fr, z)
+        for d in (0, 1):
+            @pl.when(has[d])
             def _():
-                landed(line_in.at[k, side_of[i], fr, q], sum_recv.at[k, side_of[i], fr, q])
-                part[core, k, slot] = part[core, k, slot] + line_in[k, side_of[i], fr, q]
-
-            remote(part.at[core, k, slot], line_in.at[k, side_of[i], fr, q], sum_send.at[k],
-                   sum_recv.at[k, side_of[i], fr, q], device(toward[i], y, x, core)).start()
-
-    def home(k):
-        for fr in (1, 0):
-            slot = gathered(k, fr, z)
-            for d in (0, 1):
-                @pl.when(has[d])
-                def _():
-                    landed(line_in.at[k, d, fr, z], sum_recv.at[k, d, fr, z])
-                    part[core, k, slot] = part[core, k, slot] + line_in[k, d, fr, z]
-            if fr == 1:
-                remote(part.at[core, k, slot], first_in.at[k], home_send.at[k], home_recv.at[k],
-                       first_dev).start()
+                landed(line_in.at[k, d, fr, z], sum_recv.at[k, d, fr, z])
+                part[core, k, slot] = part[core, k, slot] + line_in[k, d, fr, z]
+        if fr == 1:
+            remote(part.at[core, k, slot], first_in.at[k], home_send.at[k], home_recv.at[k],
+                   first_dev).start()
 
     def final(k):
         landed(first_in.at[k], home_recv.at[k])
@@ -396,7 +391,7 @@
 
     steps = dict(own=own, first=first, line=line, last=last, hidden=hidden, down=down, back=back,
                  sum=line_sum, home=home, final=final, drain_out=drain_out, drain_back=drain_back)
-    for name, *rest in plan():
+    for name, *rest in ORDER:
         steps[name](*rest)
 
     for j in range(CHUNKS // 2):

time: 96.7 us -> 72 us (0.74)
  Pallas kernels: 94.1 us -> 70.2 us
    pallas_call x1, Pallas kernels: 94.1 us -> 70.2 us  [ring_local(): pl.pallas_call(functools.partial(ring_kernel, zs), out_shape=jax.ShapeDty...]
where the time goes in v2:
time: 72 us; the launch traced here: 71.8 us
  Pallas kernels  70.2 us (98%)
  local copies, waits for them, and re-layouts  1.62 us (2%)
    pallas_call x1, Pallas kernels, ring_local(): pl.pallas_call(functools.partial(ring_kernel, zs), out_shape=jax.ShapeDty...  70.2 us
    unnamed x1, local copies, waits for them, and re-layouts  1.62 us

profile of v2, /device:TPU:0, one launch (start us, length us, event | category | flops | bytes accessed | tf_op | source)
XLA Modules:
  0.0 71.8 jit_solution(14568868717975039651)
XLA Ops:
  0.0 70.2 %shard_map.82 = bf16[32,3072]{1,0:T(8,128)(2,1)} custom-call(bf16[32,3072]{1,0:T(8,128)(2,1)} %tok_ref.1, f32[1,3072]{1,0:T(1,128)} %bitcast.4, s32[4,32]{1,0:T(4,128)} %bitcast.5, f32[4,32]{1,0:T(4,128)} %bitcast.6, f32[1,32]{1,0:T(1,128)} %bitcast.7, bf16[1,3072,384]{2,1,0:T(8,128)(2,1)} %gate_hbm.1, bf16[1,3072,384]{2,1,0:T(8,128)(2,1)} %up_hbm.1, ...), custom_call_target="tpu_custom_call" | custom-call | tf_op jit(solution)/shard_map/pallas_call | solution.py:436
  70.2 1.6 %copy.10 = bf16[32,3072]{1,0:T(8,128)(2,1)} copy(bf16[32,3072]{1,0:T(8,128)(2,1)} %shard_map.82) | data formatting | bytes 393216

commit v3 on v1

--- a/solution.py
+++ b/solution.py
@@ -76,31 +76,57 @@
 CHUNKS = 4
 
 
-def plan():
-    order = []
-
-    def at(time, *step):
-        order.append((time, len(order), step))
-
-    for k in range(CHUNKS):
-        base = 6.3 * k
-        at(max(base - 4.0, 0.1 * k), "own", k)
-        at(base + 2.5, "first", k)
-        for i in range(1, 4):
-            at(base + 2.5 + 2.3 * i, "line", k, i)
-        for i in range(4):
-            at(base + 4.9 + 2.3 * i, "last", k, i)
-        ready = base + 14.0
-        at(ready, "hidden", k)
-        at(ready + 1.5, "down", k)
-        at(ready + 4.0, "back", k)
-        for i in range(3):
-            at(ready + 7.5 + 2.3 * i, "sum", k, i)
-        at(ready + 14.5, "home", k)
-        at(ready + 17.0, "final", k)
-        at(ready + 8.0, "drain_out", k)
-        at(ready + 20.0, "drain_back", k)
-    return [step for _, _, step in sorted(order)]
+END_ORDER = (
+    ("own", 0), ("own", 2), ("own", 1), ("firstq", 0, 0), ("own", 3), ("line", 0, 1, 0), ("line", 2, 1, 0),
+    ("line", 1, 1, 0), ("first", 1), ("line", 0, 2, 0), ("line", 3, 1, 0), ("first", 2), ("last", 1, 0, 0),
+    ("line", 3, 2, 0), ("last", 1, 1, 0), ("firstq", 0, 1), ("firstq", 0, 2), ("line", 0, 3, 0),
+    ("last", 0, 2, 0), ("last", 2, 1, 0), ("firstq", 0, 3), ("line", 2, 1, 1), ("line", 3, 3, 0),
+    ("last", 0, 1, 1), ("firstq", 3, 1), ("last", 0, 1, 0), ("last", 0, 0, 1), ("line", 2, 2, 0),
+    ("last", 2, 0, 0), ("firstq", 3, 2), ("last", 3, 0, 0), ("last", 0, 0, 0), ("line", 2, 3, 1),
+    ("line", 1, 2, 0), ("last", 0, 2, 1), ("last", 0, 3, 0), ("last", 0, 3, 1), ("line", 2, 3, 0),
+    ("line", 2, 2, 1), ("firstq", 3, 3), ("hidden", 0), ("line", 1, 3, 1), ("last", 3, 2, 1),
+    ("last", 2, 2, 0), ("firstq", 3, 0), ("last", 3, 3, 0), ("last", 2, 0, 1), ("last", 2, 1, 1),
+    ("down", 0, 0), ("line", 1, 2, 1), ("last", 2, 3, 0), ("last", 2, 3, 1), ("last", 2, 2, 1),
+    ("last", 3, 2, 0), ("line", 1, 3, 0), ("last", 3, 1, 1), ("last", 3, 1, 0), ("line", 1, 1, 1),
+    ("down", 0, 1), ("last", 3, 3, 1), ("back", 0), ("hidden", 2), ("last", 3, 0, 1), ("last", 1, 0, 1),
+    ("last", 1, 2, 0), ("down", 2, 0), ("down", 2, 1), ("last", 1, 3, 0), ("fsum", 0, 0), ("last", 1, 1, 1),
+    ("hidden", 3), ("last", 1, 3, 1), ("last", 1, 2, 1), ("back", 2), ("down", 3, 0), ("zsum", 0, 0),
+    ("hidden", 1), ("down", 3, 1), ("fsum", 0, 1), ("back", 3), ("sum", 2, 0, 1), ("sum", 2, 1, 1),
+    ("down", 1, 0), ("zsum", 0, 1), ("sum", 2, 2, 1), ("fsum", 3, 0), ("sum", 2, 1, 0), ("sum", 2, 0, 0),
+    ("down", 1, 1), ("back", 1), ("zsum", 3, 0), ("sum", 1, 0, 1), ("sum", 1, 1, 1), ("fsum", 3, 1),
+    ("fsum", 3, 2), ("fsum", 0, 2), ("fsum", 3, 3), ("sum", 1, 0, 0), ("sum", 1, 2, 1), ("sum", 1, 1, 0),
+    ("zsum", 3, 1), ("sum", 2, 2, 0), ("home", 2, 1), ("sum", 1, 2, 0), ("zsum", 3, 2), ("zsum", 0, 2),
+    ("fsum", 0, 3), ("home", 1, 1), ("home", 2, 0), ("final", 2), ("homez", 3), ("homez", 0), ("home", 1, 0),
+    ("drain_out", 0), ("drain_out", 1), ("drain_out", 2), ("drain_out", 3), ("drain_back", 0),
+    ("drain_back", 2), ("drain_back", 3), ("final", 1), ("drain_back", 1),
+)
+
+INNER_ORDER = (
+    ("own", 2), ("own", 0), ("own", 1), ("own", 3), ("line", 0, 2, 0), ("line", 0, 1, 0), ("line", 2, 2, 0),
+    ("first", 2), ("firstq", 3, 0), ("line", 3, 1, 0), ("line", 0, 3, 0), ("line", 2, 1, 0),
+    ("line", 3, 2, 0), ("first", 1), ("firstq", 0, 0), ("line", 1, 2, 1), ("line", 3, 3, 0),
+    ("line", 2, 2, 1), ("last", 0, 2, 0), ("firstq", 0, 1), ("firstq", 3, 1), ("firstq", 0, 3),
+    ("firstq", 0, 2), ("last", 2, 0, 0), ("line", 1, 2, 0), ("last", 0, 0, 0), ("line", 1, 1, 0),
+    ("line", 1, 3, 1), ("firstq", 3, 2), ("line", 2, 3, 1), ("last", 3, 1, 0), ("line", 2, 3, 0),
+    ("last", 0, 1, 0), ("last", 3, 2, 0), ("firstq", 3, 3), ("line", 2, 1, 1), ("last", 0, 1, 1),
+    ("last", 3, 0, 1), ("last", 0, 3, 0), ("line", 1, 3, 0), ("last", 1, 2, 1), ("last", 0, 0, 1),
+    ("last", 2, 0, 1), ("last", 0, 3, 1), ("line", 1, 1, 1), ("last", 2, 2, 1), ("last", 2, 2, 0),
+    ("last", 0, 2, 1), ("last", 1, 2, 0), ("hidden", 0), ("last", 1, 3, 1), ("last", 3, 1, 1), ("down", 0, 0),
+    ("down", 0, 1), ("last", 2, 1, 0), ("last", 3, 2, 1), ("last", 3, 3, 0), ("last", 3, 3, 1),
+    ("last", 3, 0, 0), ("back", 0), ("last", 2, 1, 1), ("last", 1, 0, 0), ("last", 2, 3, 0), ("hidden", 3),
+    ("down", 3, 0), ("down", 3, 1), ("last", 1, 3, 0), ("last", 2, 3, 1), ("last", 1, 1, 0), ("fsum", 0, 0),
+    ("back", 3), ("hidden", 2), ("last", 1, 0, 1), ("last", 1, 1, 1), ("fsum", 0, 2), ("down", 2, 0),
+    ("fsum", 3, 0), ("zsum", 0, 0), ("down", 2, 1), ("back", 2), ("hidden", 1), ("down", 1, 0),
+    ("zsum", 0, 2), ("sum", 2, 0, 1), ("fsum", 3, 1), ("down", 1, 1), ("back", 1), ("sum", 2, 0, 0),
+    ("sum", 2, 2, 1), ("zsum", 3, 0), ("sum", 1, 0, 1), ("sum", 2, 1, 1), ("fsum", 3, 3), ("sum", 2, 1, 0),
+    ("sum", 1, 2, 1), ("fsum", 3, 2), ("fsum", 0, 1), ("fsum", 0, 3), ("zsum", 3, 1), ("sum", 1, 0, 0),
+    ("sum", 1, 1, 1), ("sum", 2, 2, 0), ("home", 2, 1), ("zsum", 0, 1), ("sum", 1, 2, 0), ("zsum", 3, 2),
+    ("home", 1, 1), ("sum", 1, 1, 0), ("home", 2, 0), ("home", 1, 0), ("final", 1), ("homez", 3),
+    ("final", 2), ("drain_out", 0), ("drain_out", 1), ("drain_out", 2), ("drain_out", 3), ("drain_back", 1),
+    ("drain_back", 2), ("drain_back", 3), ("homez", 0), ("drain_back", 0),
+)
+
+Z_FIRST = (True, False, False, True)
 
 
 def ring_kernel(
@@ -143,7 +169,6 @@
         planes.append(q)
     below = [q < z for q in planes]
     away = [jnp.where(b, z + 1, z - 1) for b in below]
-    away_ok = [jnp.logical_and(a >= 0, a < zs) for a in away]
     toward = [jnp.where(b, z - 1, z + 1) for b in below]
     side_of = [jnp.where(b, 1, 0) for b in below]
 
@@ -152,6 +177,7 @@
     count = tok_ref.shape[0]
     rows = stage.shape[1]
     blocks = 4 * zs
+    inner = hid.shape[2]
 
     copies = [
         pltpu.make_async_copy(gate_hbm.at[0], wgu.at[:, : wgu.shape[1] // 2], w_sem.at[0]),
@@ -239,50 +265,78 @@
         remote(stage.at[j], xg.at[core * 0 + other, k, own_slot, :, pl.ds(0, half)],
                stage_send.at[j], stage_recv.at[k], partner).start()
 
-    def spread(k, slot, fr, i):
-        ref = block(core, k, slot)
-        sem = gather_recv.at[k, slot]
-        if i == 0:
-            for d in (0, 1):
-                @pl.when(has[d])
-                def _():
-                    remote(ref, ref, own_send.at[k, d], sem, device(z - 1 + 2 * d, y, x, core)).start()
-        else:
-            @pl.when(away_ok[i])
+    onward = jnp.where(z == 0, 1, z - 1)
+
+    def program(at_end, order):
+        sides = (jnp.where(z == 0, 1, 0),) if at_end else (0, 1)
+
+        def out_z(ref, k, slot, sem_of):
+            for n, d in enumerate((onward,) if at_end else (z - 1, z + 1)):
+                remote(ref, ref, sem_of(n), gather_recv.at[k, slot], device(d, y, x, core)).start()
+
+        def spread(k, fr, i):
+            slot = cols[fr][0] + planes[i]
+            ref = block(core, k, slot)
+            sem = gather_recv.at[k, slot]
+            if i == 0:
+                out_z(ref, k, slot, lambda n: own_send.at[k, n])
+            elif not at_end:
+                remote(ref, ref, line_send.at[k, i], sem, device(away[i], y, x, core)).start()
+            if Z_FIRST[k] and fr == 0:
+                remote(ref, ref, first_send.at[k], sem, first_dev).start()
+            remote(ref, ref, last_send.at[k], sem, last_dev).start()
+            remote(ref, ref, mate_send.at[k], mate_recv.at[k], partner).start()
+
+        def own(k):
+            @pl.when(core != k % 2)
             def _():
-                remote(ref, ref, line_send.at[k, i], sem, device(away[i], y, x, core)).start()
-        remote(ref, ref, last_send.at[k], sem, last_dev).start()
-        remote(ref, ref, mate_send.at[k], mate_recv.at[k], partner).start()
-
-    def own(k):
-        @pl.when(core != k % 2)
-        def _():
-            landed(xg.at[core, k, own_slot, :, pl.ds(0, half)], stage_recv.at[k])
-        ref = block(core, k, own_slot)
-        remote(ref, ref, first_send.at[k], gather_recv.at[k, own_slot], first_dev).start()
-        spread(k, own_slot, 0, 0)
-
-    def first(k):
-        slot = cols[1][0] + z
-        landed(block(core, k, slot), gather_recv.at[k, slot])
-        spread(k, slot, 1, 0)
-
-    def line(k, i):
-        for fr in (0, 1):
-            slot = cols[fr][0] + planes[i]
-            landed(block(core, k, slot), gather_recv.at[k, slot])
-            spread(k, slot, fr, i)
-
-    def last(k, i):
-        for fr in (0, 1):
-            slot = cols[fr][1] + planes[i]
+                landed(xg.at[core, k, own_slot, :, pl.ds(0, half)], stage_recv.at[k])
+            if not Z_FIRST[k]:
+                ref = block(core, k, own_slot)
+                remote(ref, ref, first_send.at[k], gather_recv.at[k, own_slot], first_dev).start()
+            spread(k, 0, 0)
+
+        def arrived(k, fr, lr, i):
+            slot = cols[fr][lr] + planes[i]
             ref = block(core, k, slot)
             landed(ref, gather_recv.at[k, slot])
+            return ref, slot
+
+        def first(k):
+            arrived(k, 1, 0, 0)
+            spread(k, 1, 0)
+
+        def line(k, i, fr):
+            arrived(k, fr, 0, i)
+            spread(k, fr, i)
+
+        def firstq(k, i):
+            ref, slot = arrived(k, 1, 0, i)
+            remote(ref, ref, last_send.at[k], gather_recv.at[k, slot], last_dev).start()
             remote(ref, ref, mate_send.at[k], mate_recv.at[k], partner).start()
 
-    def hidden(k):
-        landed(span(other, k, blocks), mate_recv.at[k])
-        if k == 0:
+        def last(k, i, fr):
+            ref, slot = arrived(k, fr, 1, i)
+            remote(ref, ref, mate_send.at[k], mate_recv.at[k], partner).start()
+
+        def hidden(k):
+            landed(span(other, k, blocks), mate_recv.at[k])
+            if order[[o[0] for o in order].index("hidden")][1] == k:
+                start_compute()
+            shape = (blocks, rows, LANES)
+            pick = lax.broadcasted_iota(jnp.int32, shape, 2) == (
+                lax.broadcasted_iota(jnp.int32, shape, 1) + rows * (k // 2))
+            scale = jnp.sum(jnp.where(pick, scales[k % 2][:, None, :], 0.0), axis=2, keepdims=True)
+            scale = scale.reshape(blocks * rows, 1)
+            left = xg[0, k, :, :, :half].reshape(blocks * rows, half)
+            right = xg[1, k, :, :, :half].reshape(blocks * rows, half)
+            acts = jnp.dot(left, wgu[:half, :], preferred_element_type=jnp.float32) + jnp.dot(
+                right, wgu[half:, :], preferred_element_type=jnp.float32
+            )
+            value = jax.nn.silu(acts[:, :inner]) * acts[:, inner:] * scale
+            hid[k] = value.astype(jnp.bfloat16)
+
+        def start_compute():
             for copy in copies:
                 copy.wait()
             expert = me.astype(jnp.float32)
@@ -293,111 +347,111 @@
                     value = tags[:, TOP_K + n, :] + tags[:, 2 * TOP_K + n, :]
                     scale += jnp.where(tags[:, n, :] == expert, value, 0.0)
                 scales[h] = scale
-        shape = (blocks, rows, LANES)
-        pick = lax.broadcasted_iota(jnp.int32, shape, 2) == (
-            lax.broadcasted_iota(jnp.int32, shape, 1) + rows * (k // 2))
-        scale = jnp.sum(jnp.where(pick, scales[k % 2][:, None, :], 0.0), axis=2, keepdims=True)
-        scale = scale.reshape(blocks * rows, 1)
-        left = xg[0, k, :, :, :half].reshape(blocks * rows, half)
-        right = xg[1, k, :, :, :half].reshape(blocks * rows, half)
-        acts = jnp.dot(left, wgu[:half, :], preferred_element_type=jnp.float32) + jnp.dot(
-            right, wgu[half:, :], preferred_element_type=jnp.float32
-        )
-        inner = hid.shape[1]
-        hid[...] = (jax.nn.silu(acts[:, :inner]) * acts[:, inner:] * scale).astype(jnp.bfloat16)
-
-    def down(k):
-        step = half // 3 if half % (3 * LANES) == 0 else half
-        for h in (other, core):
+
+        def down(k, i):
+            step = half // 3 if half % (3 * LANES) == 0 else half
+            h = core if i else other
             for at in range(0, half, step):
-                out = jnp.dot(hid[...], wd[h, :, at : at + step], preferred_element_type=jnp.float32)
+                out = jnp.dot(hid[k], wd[h, :, at : at + step], preferred_element_type=jnp.float32)
                 part[h, k, :, :, at : at + step] = out.astype(jnp.bfloat16).reshape(blocks, rows, step)
-            if h is other:
+            if i == 0:
                 remote(part.at[other, k], pair_in.at[k], pair_send.at[k], pair_recv.at[k], partner).start()
 
-    def back(k):
-        landed(pair_in.at[k], pair_recv.at[k])
-        for i in range(zs - 1, -1, -1):
-            for fr in (0, 1):
-                slot = cols[fr][1] + planes[i]
-                part[core, k, slot] = part[core, k, slot] + pair_in[k, slot]
-                remote(part.at[core, k, slot], last_in.at[k, fr, planes[i]], back_send.at[k],
-                       back_recv.at[k, fr, planes[i]], last_dev).start()
-
-    def gathered(k, fr, q):
-        slot = cols[fr][0] + q
-        landed(last_in.at[k, fr, q], back_recv.at[k, fr, q])
-        held = part[core, k, slot].astype(jnp.float32) + pair_in[k, slot].astype(jnp.float32)
-        part[core, k, slot] = (held + last_in[k, fr, q].astype(jnp.float32)).astype(jnp.bfloat16)
-        return slot
-
-    def line_sum(k, j):
-        i = zs - 1 - j
-        q = planes[i]
-        for fr in (0, 1):
-            slot = gathered(k, fr, q)
-
-            @pl.when(away_ok[i])
-            def _():
-                landed(line_in.at[k, side_of[i], fr, q], sum_recv.at[k, side_of[i], fr, q])
-                part[core, k, slot] = part[core, k, slot] + line_in[k, side_of[i], fr, q]
-
+        def back(k):
+            landed(pair_in.at[k], pair_recv.at[k])
+            for i in range(zs - 1, -1, -1):
+                for fr in (0, 1):
+                    slot = cols[fr][1] + planes[i]
+                    part[core, k, slot] = part[core, k, slot] + pair_in[k, slot]
+                    remote(part.at[core, k, slot], last_in.at[k, fr, planes[i]], back_send.at[k],
+                           back_recv.at[k, fr, planes[i]], last_dev).start()
+
+        def collect(k, fr, q, from_line=(), from_first=False):
+            slot = cols[fr][0] + q
+            landed(last_in.at[k, fr, q], back_recv.at[k, fr, q])
+            held = part[core, k, slot].astype(jnp.float32) + pair_in[k, slot].astype(jnp.float32)
+            held = held + last_in[k, fr, q].astype(jnp.float32)
+            if from_first:
+                landed(first_in.at[k, q], home_recv.at[k, q])
+                held = held + first_in[k, q].astype(jnp.float32)
+            for side in from_line:
+                landed(line_in.at[k, side, fr, q], sum_recv.at[k, side, fr, q])
+                held = held + line_in[k, side, fr, q].astype(jnp.float32)
+            part[core, k, slot] = held.astype(jnp.bfloat16)
+            return slot
+
+        def line_sum(k, j, fr):
+            i = zs - 1 - j
+            q = planes[i]
+            slot = collect(k, fr, q, () if at_end else (side_of[i],), Z_FIRST[k])
             remote(part.at[core, k, slot], line_in.at[k, side_of[i], fr, q], sum_send.at[k],
                    sum_recv.at[k, side_of[i], fr, q], device(toward[i], y, x, core)).start()
 
-    def home(k):
-        for fr in (1, 0):
-            slot = gathered(k, fr, z)
-            for d in (0, 1):
-                @pl.when(has[d])
-                def _():
-                    landed(line_in.at[k, d, fr, z], sum_recv.at[k, d, fr, z])
-                    part[core, k, slot] = part[core, k, slot] + line_in[k, d, fr, z]
+        def zsum(k, j):
+            line_sum(k, j, 0)
+
+        def to_first(k, slot, q):
+            remote(part.at[core, k, slot], first_in.at[k, q], home_send.at[k], home_recv.at[k, q],
+                   first_dev).start()
+
+        def fsum(k, j):
+            q = planes[zs - 1 - j]
+            to_first(k, collect(k, 1, q), q)
+
+        def home(k, fr):
+            slot = collect(k, fr, z, sides)
             if fr == 1:
-                remote(part.at[core, k, slot], first_in.at[k], home_send.at[k], home_recv.at[k],
-                       first_dev).start()
-
-    def final(k):
-        landed(first_in.at[k], home_recv.at[k])
-        total = part[core, k, own_slot] + first_in[k]
-        j = k // 2
-
-        @pl.when(core == k % 2)
-        def _():
-            out_ref[j * rows : (j + 1) * rows, pl.ds(pl.multiple_of(core * half, LANES), half)] = total
-
-        @pl.when(core != k % 2)
-        def _():
+                to_first(k, slot, z)
+
+        def finish(k, total):
+            j = k // 2
+
+            @pl.when(core == k % 2)
+            def _():
+                out_ref[j * rows : (j + 1) * rows, pl.ds(pl.multiple_of(core * half, LANES), half)] = total
+
+            @pl.when(core != k % 2)
+            def _():
+                remote(part.at[core, k, own_slot], fin_in.at[j], fin_send.at[j], fin_recv.at[j],
+                       partner).start()
+
+        def final(k):
+            landed(first_in.at[k, z], home_recv.at[k, z])
+            total = part[core, k, own_slot] + first_in[k, z]
             part[core, k, own_slot] = total
-            remote(part.at[core, k, own_slot], fin_in.at[j], fin_send.at[j], fin_recv.at[j],
-                   partner).start()
-
-    def drain_out(k):
-        @pl.when(core == k % 2)
-        def _():
-            sent(stage.at[k // 2], stage_send.at[k // 2])
-        sent(block(core, k, own_slot), first_send.at[k])
-        for d in (0, 1):
-            @pl.when(has[d])
+            finish(k, total)
+
+        def homez(k):
+            collect(k, 0, z, sides, True)
+            finish(k, part[core, k, own_slot])
+
+        def drain_out(k):
+            @pl.when(core == k % 2)
             def _():
-                sent(span(core, k, 2), own_send.at[k, d])
-        for i in range(1, zs):
-            @pl.when(away_ok[i])
-            def _():
-                sent(span(core, k, 2), line_send.at[k, i])
-        sent(span(core, k, 2 * zs), last_send.at[k])
-        sent(span(core, k, blocks), mate_send.at[k])
-
-    def drain_back(k):
-        sent(part.at[other, k], pair_send.at[k])
-        sent(part.at[core, k, pl.ds(0, 2 * zs)], back_send.at[k])
-        sent(part.at[core, k, pl.ds(0, 2 * (zs - 1))], sum_send.at[k])
-        sent(part.at[core, k, 0], home_send.at[k])
-
-    steps = dict(own=own, first=first, line=line, last=last, hidden=hidden, down=down, back=back,
-                 sum=line_sum, home=home, final=final, drain_out=drain_out, drain_back=drain_back)
-    for name, *rest in plan():
-        steps[name](*rest)
+                sent(stage.at[k // 2], stage_send.at[k // 2])
+            wide_z = 1 if Z_FIRST[k] else 2
+            sent(span(core, k, zs if Z_FIRST[k] else 1), first_send.at[k])
+            for n in (0,) if at_end else (0, 1):
+                sent(span(core, k, wide_z), own_send.at[k, n])
+            for i in () if at_end else range(1, zs):
+                sent(span(core, k, wide_z), line_send.at[k, i])
+            sent(span(core, k, 2 * zs), last_send.at[k])
+            sent(span(core, k, blocks), mate_send.at[k])
+
+        def drain_back(k):
+            sent(part.at[other, k], pair_send.at[k])
+            sent(part.at[core, k, pl.ds(0, 2 * zs)], back_send.at[k])
+            sent(part.at[core, k, pl.ds(0, (1 if Z_FIRST[k] else 2) * (zs - 1))], sum_send.at[k])
+            sent(part.at[core, k, pl.ds(0, zs if Z_FIRST[k] else 1)], home_send.at[k])
+
+        steps = dict(own=own, first=first, line=line, firstq=firstq, last=last, hidden=hidden, down=down,
+                     back=back, sum=line_sum, zsum=zsum, fsum=fsum, home=home, homez=homez, final=final,
+                     drain_out=drain_out, drain_back=drain_back)
+        for name, *rest in order:
+            steps[name](*rest)
+
+    pl.when(inside)(lambda: program(False, INNER_ORDER))
+    pl.when(jnp.logical_not(inside))(lambda: program(True, END_ORDER))
 
     for j in range(CHUNKS // 2):
         landed(fin_in.at[j], fin_recv.at[j])
@@ -426,9 +480,9 @@
         pltpu.VMEM((c, blocks, rows, half), kind),
         pltpu.VMEM((c, 2, zs, rows, half), kind),
         pltpu.VMEM((c, 2, 2, zs, rows, half), kind),
-        pltpu.VMEM((c, rows, half), kind),
+        pltpu.VMEM((c, zs, rows, half), kind),
         pltpu.VMEM((c // 2, rows, half), kind),
-        pltpu.VMEM((blocks * rows, inner), kind),
+        pltpu.VMEM((c, blocks * rows, inner), kind),
         pltpu.VMEM((2, blocks, LANES), jnp.float32),
         pltpu.VMEM((width, 2 * inner), kind),
         pltpu.VMEM((2, inner, half), kind),
@@ -436,7 +490,7 @@
         dma((c // 2,)), dma((c,)), dma((c, blocks)), dma((c, 2)), dma((c,)), dma((c, zs)), dma((c,)),
         dma((c,)), dma((c,)), dma((c,)), dma((c,)), dma((c,)), dma((c, 2, zs)),
         dma((c,)), dma((c, 2, 2, zs)),
-        dma((c,)), dma((c,)), dma((c // 2,)), dma((c // 2,)),
+        dma((c,)), dma((c, zs)), dma((c // 2,)), dma((c // 2,)),
     ]
     return pl.pallas_call(
         functools.partial(ring_kernel, zs),

time: 96.7 us -> 67.9 us (0.70)
  Pallas kernels: 94.1 us -> 66.2 us
    pallas_call x1, Pallas kernels: 94.1 us -> 66.2 us  [ring_local(): pl.pallas_call(functools.partial(ring_kernel, zs), out_shape=jax.ShapeDty...]
where the time goes in v3:
time: 67.9 us; the launch traced here: 67.8 us
  Pallas kernels  66.2 us (97%)
  local copies, waits for them, and re-layouts  1.62 us (2%)
    pallas_call x1, Pallas kernels, ring_local(): pl.pallas_call(functools.partial(ring_kernel, zs), out_shape=jax.ShapeDty...  66.2 us
    unnamed x1, local copies, waits for them, and re-layouts  1.62 us

profile of v3, /device:TPU:0, one launch (start us, length us, event | category | flops | bytes accessed | tf_op | source)
XLA Modules:
  0.0 67.8 jit_solution(15757354708844799685)
XLA Ops:
  0.0 66.2 %shard_map.82 = bf16[32,3072]{1,0:T(8,128)(2,1)} custom-call(bf16[32,3072]{1,0:T(8,128)(2,1)} %tok_ref.1, f32[1,3072]{1,0:T(1,128)} %bitcast.4, s32[4,32]{1,0:T(4,128)} %bitcast.5, f32[4,32]{1,0:T(4,128)} %bitcast.6, f32[1,32]{1,0:T(1,128)} %bitcast.7, bf16[1,3072,384]{2,1,0:T(8,128)(2,1)} %gate_hbm.1, bf16[1,3072,384]{2,1,0:T(8,128)(2,1)} %up_hbm.1, ...), custom_call_target="tpu_custom_call" | custom-call | tf_op jit(solution)/shard_map/pallas_call | solution.py:495
  66.2 1.6 %copy.10 = bf16[32,3072]{1,0:T(8,128)(2,1)} copy(bf16[32,3072]{1,0:T(8,128)(2,1)} %shard_map.82) | data formatting | bytes 393216

commit v4 on v3

--- a/solution.py
+++ b/solution.py
@@ -77,56 +77,57 @@
 
 
 END_ORDER = (
-    ("own", 0), ("own", 2), ("own", 1), ("firstq", 0, 0), ("own", 3), ("line", 0, 1, 0), ("line", 2, 1, 0),
-    ("line", 1, 1, 0), ("first", 1), ("line", 0, 2, 0), ("line", 3, 1, 0), ("first", 2), ("last", 1, 0, 0),
-    ("line", 3, 2, 0), ("last", 1, 1, 0), ("firstq", 0, 1), ("firstq", 0, 2), ("line", 0, 3, 0),
-    ("last", 0, 2, 0), ("last", 2, 1, 0), ("firstq", 0, 3), ("line", 2, 1, 1), ("line", 3, 3, 0),
-    ("last", 0, 1, 1), ("firstq", 3, 1), ("last", 0, 1, 0), ("last", 0, 0, 1), ("line", 2, 2, 0),
-    ("last", 2, 0, 0), ("firstq", 3, 2), ("last", 3, 0, 0), ("last", 0, 0, 0), ("line", 2, 3, 1),
-    ("line", 1, 2, 0), ("last", 0, 2, 1), ("last", 0, 3, 0), ("last", 0, 3, 1), ("line", 2, 3, 0),
-    ("line", 2, 2, 1), ("firstq", 3, 3), ("hidden", 0), ("line", 1, 3, 1), ("last", 3, 2, 1),
-    ("last", 2, 2, 0), ("firstq", 3, 0), ("last", 3, 3, 0), ("last", 2, 0, 1), ("last", 2, 1, 1),
-    ("down", 0, 0), ("line", 1, 2, 1), ("last", 2, 3, 0), ("last", 2, 3, 1), ("last", 2, 2, 1),
-    ("last", 3, 2, 0), ("line", 1, 3, 0), ("last", 3, 1, 1), ("last", 3, 1, 0), ("line", 1, 1, 1),
-    ("down", 0, 1), ("last", 3, 3, 1), ("back", 0), ("hidden", 2), ("last", 3, 0, 1), ("last", 1, 0, 1),
-    ("last", 1, 2, 0), ("down", 2, 0), ("down", 2, 1), ("last", 1, 3, 0), ("fsum", 0, 0), ("last", 1, 1, 1),
-    ("hidden", 3), ("last", 1, 3, 1), ("last", 1, 2, 1), ("back", 2), ("down", 3, 0), ("zsum", 0, 0),
-    ("hidden", 1), ("down", 3, 1), ("fsum", 0, 1), ("back", 3), ("sum", 2, 0, 1), ("sum", 2, 1, 1),
-    ("down", 1, 0), ("zsum", 0, 1), ("sum", 2, 2, 1), ("fsum", 3, 0), ("sum", 2, 1, 0), ("sum", 2, 0, 0),
-    ("down", 1, 1), ("back", 1), ("zsum", 3, 0), ("sum", 1, 0, 1), ("sum", 1, 1, 1), ("fsum", 3, 1),
-    ("fsum", 3, 2), ("fsum", 0, 2), ("fsum", 3, 3), ("sum", 1, 0, 0), ("sum", 1, 2, 1), ("sum", 1, 1, 0),
-    ("zsum", 3, 1), ("sum", 2, 2, 0), ("home", 2, 1), ("sum", 1, 2, 0), ("zsum", 3, 2), ("zsum", 0, 2),
-    ("fsum", 0, 3), ("home", 1, 1), ("home", 2, 0), ("final", 2), ("homez", 3), ("homez", 0), ("home", 1, 0),
+    ("own", 0), ("own", 3), ("own", 2), ("firstq", 0, 0), ("own", 1), ("first", 3), ("line", 2, 1, 0),
+    ("line", 0, 1, 0), ("line", 3, 1, 0), ("firstq", 2, 1), ("line", 0, 2, 0), ("line", 0, 3, 0),
+    ("line", 1, 1, 1), ("last", 0, 0, 0), ("firstq", 0, 2), ("last", 0, 1, 0), ("firstq", 0, 1), ("first", 1),
+    ("last", 2, 1, 1), ("last", 0, 2, 0), ("firstq", 0, 3), ("last", 0, 3, 0), ("line", 3, 2, 0),
+    ("last", 3, 1, 0), ("line", 3, 1, 1), ("line", 3, 3, 1), ("last", 1, 1, 1), ("line", 3, 3, 0),
+    ("last", 0, 1, 1), ("last", 0, 2, 1), ("line", 3, 2, 1), ("last", 0, 0, 1), ("last", 0, 3, 1),
+    ("last", 2, 1, 0), ("last", 2, 0, 0), ("line", 1, 1, 0), ("last", 3, 0, 1), ("line", 2, 3, 0),
+    ("line", 2, 2, 0), ("firstq", 2, 0), ("hidden", 0), ("last", 3, 1, 1), ("line", 1, 2, 0),
+    ("last", 3, 2, 1), ("last", 3, 3, 0), ("last", 3, 0, 0), ("last", 1, 0, 1), ("last", 3, 3, 1),
+    ("last", 3, 2, 0), ("down", 0, 0), ("line", 1, 2, 1), ("line", 1, 3, 0), ("last", 2, 3, 0),
+    ("line", 1, 3, 1), ("firstq", 2, 2), ("last", 2, 2, 0), ("firstq", 2, 3), ("down", 0, 1),
+    ("last", 1, 1, 0), ("back", 0), ("last", 2, 0, 1), ("last", 1, 0, 0), ("hidden", 3), ("last", 1, 2, 1),
+    ("last", 1, 3, 0), ("last", 1, 2, 0), ("last", 1, 3, 1), ("down", 3, 0), ("hidden", 1), ("fsum", 0, 0),
+    ("down", 3, 1), ("back", 3), ("down", 1, 0), ("last", 2, 3, 1), ("last", 2, 2, 1), ("zsum", 0, 0),
+    ("down", 1, 1), ("back", 1), ("sum", 3, 0, 0), ("sum", 3, 0, 1), ("sum", 3, 1, 0), ("hidden", 2),
+    ("down", 2, 0), ("sum", 3, 2, 1), ("sum", 3, 1, 1), ("down", 2, 1), ("back", 2), ("sum", 1, 0, 1),
+    ("sum", 1, 0, 0), ("sum", 1, 1, 1), ("sum", 1, 2, 1), ("sum", 3, 2, 0), ("fsum", 2, 0), ("fsum", 2, 1),
+    ("sum", 1, 1, 0), ("fsum", 0, 1), ("zsum", 2, 0), ("fsum", 2, 3), ("zsum", 2, 1), ("home", 3, 1),
+    ("fsum", 2, 2), ("zsum", 0, 1), ("sum", 1, 2, 0), ("fsum", 0, 2), ("home", 1, 1), ("home", 3, 0),
+    ("zsum", 2, 2), ("final", 3), ("home", 1, 0), ("fsum", 0, 3), ("zsum", 0, 2), ("final", 1), ("homez", 0),
     ("drain_out", 0), ("drain_out", 1), ("drain_out", 2), ("drain_out", 3), ("drain_back", 0),
-    ("drain_back", 2), ("drain_back", 3), ("final", 1), ("drain_back", 1),
+    ("drain_back", 1), ("drain_back", 3), ("homez", 2), ("drain_back", 2),
 )
 
 INNER_ORDER = (
-    ("own", 2), ("own", 0), ("own", 1), ("own", 3), ("line", 0, 2, 0), ("line", 0, 1, 0), ("line", 2, 2, 0),
-    ("first", 2), ("firstq", 3, 0), ("line", 3, 1, 0), ("line", 0, 3, 0), ("line", 2, 1, 0),
-    ("line", 3, 2, 0), ("first", 1), ("firstq", 0, 0), ("line", 1, 2, 1), ("line", 3, 3, 0),
-    ("line", 2, 2, 1), ("last", 0, 2, 0), ("firstq", 0, 1), ("firstq", 3, 1), ("firstq", 0, 3),
-    ("firstq", 0, 2), ("last", 2, 0, 0), ("line", 1, 2, 0), ("last", 0, 0, 0), ("line", 1, 1, 0),
-    ("line", 1, 3, 1), ("firstq", 3, 2), ("line", 2, 3, 1), ("last", 3, 1, 0), ("line", 2, 3, 0),
-    ("last", 0, 1, 0), ("last", 3, 2, 0), ("firstq", 3, 3), ("line", 2, 1, 1), ("last", 0, 1, 1),
-    ("last", 3, 0, 1), ("last", 0, 3, 0), ("line", 1, 3, 0), ("last", 1, 2, 1), ("last", 0, 0, 1),
-    ("last", 2, 0, 1), ("last", 0, 3, 1), ("line", 1, 1, 1), ("last", 2, 2, 1), ("last", 2, 2, 0),
-    ("last", 0, 2, 1), ("last", 1, 2, 0), ("hidden", 0), ("last", 1, 3, 1), ("last", 3, 1, 1), ("down", 0, 0),
-    ("down", 0, 1), ("last", 2, 1, 0), ("last", 3, 2, 1), ("last", 3, 3, 0), ("last", 3, 3, 1),
-    ("last", 3, 0, 0), ("back", 0), ("last", 2, 1, 1), ("last", 1, 0, 0), ("last", 2, 3, 0), ("hidden", 3),
-    ("down", 3, 0), ("down", 3, 1), ("last", 1, 3, 0), ("last", 2, 3, 1), ("last", 1, 1, 0), ("fsum", 0, 0),
-    ("back", 3), ("hidden", 2), ("last", 1, 0, 1), ("last", 1, 1, 1), ("fsum", 0, 2), ("down", 2, 0),
-    ("fsum", 3, 0), ("zsum", 0, 0), ("down", 2, 1), ("back", 2), ("hidden", 1), ("down", 1, 0),
-    ("zsum", 0, 2), ("sum", 2, 0, 1), ("fsum", 3, 1), ("down", 1, 1), ("back", 1), ("sum", 2, 0, 0),
-    ("sum", 2, 2, 1), ("zsum", 3, 0), ("sum", 1, 0, 1), ("sum", 2, 1, 1), ("fsum", 3, 3), ("sum", 2, 1, 0),
-    ("sum", 1, 2, 1), ("fsum", 3, 2), ("fsum", 0, 1), ("fsum", 0, 3), ("zsum", 3, 1), ("sum", 1, 0, 0),
-    ("sum", 1, 1, 1), ("sum", 2, 2, 0), ("home", 2, 1), ("zsum", 0, 1), ("sum", 1, 2, 0), ("zsum", 3, 2),
-    ("home", 1, 1), ("sum", 1, 1, 0), ("home", 2, 0), ("home", 1, 0), ("final", 1), ("homez", 3),
-    ("final", 2), ("drain_out", 0), ("drain_out", 1), ("drain_out", 2), ("drain_out", 3), ("drain_back", 1),
-    ("drain_back", 2), ("drain_back", 3), ("homez", 0), ("drain_back", 0),
+    ("own", 0), ("own", 2), ("own", 1), ("own", 3), ("line", 0, 2, 0), ("line", 0, 1, 0), ("line", 2, 1, 0),
+    ("line", 3, 2, 0), ("first", 1), ("line", 0, 3, 0), ("firstq", 0, 0), ("firstq", 0, 2), ("line", 3, 3, 0),
+    ("firstq", 0, 1), ("line", 3, 2, 1), ("first", 3), ("firstq", 0, 3), ("line", 3, 1, 0), ("last", 0, 2, 0),
+    ("line", 3, 3, 1), ("line", 2, 2, 0), ("firstq", 2, 1), ("last", 2, 0, 0), ("line", 1, 2, 0),
+    ("line", 3, 1, 1), ("last", 0, 1, 0), ("line", 2, 3, 0), ("line", 1, 1, 0), ("line", 1, 1, 1),
+    ("last", 0, 2, 1), ("last", 0, 0, 0), ("last", 3, 0, 0), ("line", 1, 3, 0), ("last", 0, 0, 1),
+    ("line", 1, 2, 1), ("firstq", 2, 0), ("last", 3, 0, 1), ("last", 0, 3, 0), ("last", 3, 3, 0),
+    ("last", 0, 1, 1), ("last", 1, 0, 0), ("firstq", 2, 3), ("last", 3, 2, 1), ("last", 0, 3, 1),
+    ("last", 3, 1, 0), ("firstq", 2, 2), ("line", 1, 3, 1), ("hidden", 0), ("last", 1, 0, 1),
+    ("last", 3, 3, 1), ("down", 0, 0), ("down", 0, 1), ("last", 2, 1, 1), ("last", 3, 1, 1),
+    ("last", 3, 2, 0), ("back", 0), ("last", 2, 2, 0), ("last", 2, 3, 0), ("hidden", 3), ("last", 2, 0, 1),
+    ("last", 1, 2, 1), ("last", 2, 2, 1), ("last", 2, 3, 1), ("last", 2, 1, 0), ("down", 3, 0), ("hidden", 2),
+    ("last", 1, 1, 0), ("down", 3, 1), ("fsum", 0, 0), ("back", 3), ("last", 1, 1, 1), ("last", 1, 3, 1),
+    ("down", 2, 0), ("last", 1, 3, 0), ("down", 2, 1), ("last", 1, 2, 0), ("back", 2), ("hidden", 1),
+    ("down", 1, 0), ("sum", 3, 0, 0), ("down", 1, 1), ("sum", 3, 0, 1), ("back", 1), ("sum", 3, 2, 0),
+    ("sum", 3, 2, 1), ("sum", 1, 0, 0), ("sum", 3, 1, 0), ("fsum", 0, 2), ("fsum", 2, 0), ("sum", 1, 0, 1),
+    ("sum", 3, 1, 1), ("fsum", 2, 2), ("zsum", 0, 0), ("sum", 1, 1, 0), ("fsum", 2, 3), ("sum", 1, 2, 1),
+    ("sum", 1, 1, 1), ("fsum", 0, 1), ("fsum", 2, 1), ("zsum", 2, 0), ("fsum", 0, 3), ("sum", 1, 2, 0),
+    ("home", 3, 1), ("zsum", 0, 1), ("zsum", 2, 2), ("home", 1, 1), ("zsum", 0, 2), ("zsum", 2, 1),
+    ("home", 1, 0), ("final", 1), ("home", 3, 0), ("final", 3), ("homez", 0), ("drain_out", 0),
+    ("drain_out", 1), ("drain_out", 2), ("drain_out", 3), ("drain_back", 0), ("drain_back", 1),
+    ("drain_back", 3), ("homez", 2), ("drain_back", 2),
 )
 
-Z_FIRST = (True, False, False, True)
+Z_FIRST_OUT = (True, False, True, False)
+Z_LAST_BACK = (True, False, True, False)
 
 
 def ring_kernel(
@@ -282,7 +283,7 @@
                 out_z(ref, k, slot, lambda n: own_send.at[k, n])
             elif not at_end:
                 remote(ref, ref, line_send.at[k, i], sem, device(away[i], y, x, core)).start()
-            if Z_FIRST[k] and fr == 0:
+            if Z_FIRST_OUT[k] and fr == 0:
                 remote(ref, ref, first_send.at[k], sem, first_dev).start()
             remote(ref, ref, last_send.at[k], sem, last_dev).start()
             remote(ref, ref, mate_send.at[k], mate_recv.at[k], partner).start()
@@ -291,7 +292,7 @@
             @pl.when(core != k % 2)
             def _():
                 landed(xg.at[core, k, own_slot, :, pl.ds(0, half)], stage_recv.at[k])
-            if not Z_FIRST[k]:
+            if not Z_FIRST_OUT[k]:
                 ref = block(core, k, own_slot)
                 remote(ref, ref, first_send.at[k], gather_recv.at[k, own_slot], first_dev).start()
             spread(k, 0, 0)
@@ -383,7 +384,7 @@
         def line_sum(k, j, fr):
             i = zs - 1 - j
             q = planes[i]
-            slot = collect(k, fr, q, () if at_end else (side_of[i],), Z_FIRST[k])
+            slot = collect(k, fr, q, () if at_end else (side_of[i],), Z_LAST_BACK[k])
             remote(part.at[core, k, slot], line_in.at[k, side_of[i], fr, q], sum_send.at[k],
                    sum_recv.at[k, side_of[i], fr, q], device(toward[i], y, x, core)).start()
 
@@ -429,8 +430,8 @@
             @pl.when(core == k % 2)
             def _():
                 sent(stage.at[k // 2], stage_send.at[k // 2])
-            wide_z = 1 if Z_FIRST[k] else 2
-            sent(span(core, k, zs if Z_FIRST[k] else 1), first_send.at[k])
+            wide_z = 1 if Z_FIRST_OUT[k] else 2
+            sent(span(core, k, zs if Z_FIRST_OUT[k] else 1), first_send.at[k])
             for n in (0,) if at_end else (0, 1):
                 sent(span(core, k, wide_z), own_send.at[k, n])
             for i in () if at_end else range(1, zs):
@@ -441,8 +442,8 @@
         def drain_back(k):
             sent(part.at[other, k], pair_send.at[k])
             sent(part.at[core, k, pl.ds(0, 2 * zs)], back_send.at[k])
-            sent(part.at[core, k, pl.ds(0, (1 if Z_FIRST[k] else 2) * (zs - 1))], sum_send.at[k])
-            sent(part.at[core, k, pl.ds(0, zs if Z_FIRST[k] else 1)], home_send.at[k])
+            sent(part.at[core, k, pl.ds(0, (1 if Z_LAST_BACK[k] else 2) * (zs - 1))], sum_send.at[k])
+            sent(part.at[core, k, pl.ds(0, zs if Z_LAST_BACK[k] else 1)], home_send.at[k])
 
         steps = dict(own=own, first=first, line=line, firstq=firstq, last=last, hidden=hidden, down=down,
                      back=back, sum=line_sum, zsum=zsum, fsum=fsum, home=home, homez=homez, final=final,
@@ -494,7 +495,7 @@
     ]
     return pl.pallas_call(
         functools.partial(ring_kernel, zs),
-        out_shape=jax.ShapeDtypeStruct((count, width), kind),
+        out_shape=pltpu.VMEM((count, width), kind),
         in_specs=[vmem] * 5 + [hbm] * 3,
         out_specs=vmem,
         scratch_shapes=scratch,

time: 67.9 us -> 64.2 us (0.946)
  Pallas kernels: 66.2 us -> 63.3 us
  local copies, waits for them, and re-layouts: 1.62 us -> 0.68 us
    pallas_call x1, Pallas kernels: 66.2 us -> 63.3 us  [ring_local(): pl.pallas_call(functools.partial(ring_kernel, zs), out_shape=pltpu.VMEM((...]
    unnamed x1, local copies, waits for them, and re-layouts: 1.62 us -> 0.68 us
where the time goes in v4:
time: 64.2 us; the launch traced here: 64 us
  Pallas kernels  63.3 us (99%)
  local copies, waits for them, and re-layouts  0.68 us (1%)
    pallas_call x1, Pallas kernels, ring_local(): pl.pallas_call(functools.partial(ring_kernel, zs), out_shape=pltpu.VMEM((...  63.3 us

profile of v4, /device:TPU:0, one launch (start us, length us, event | category | flops | bytes accessed | tf_op | source)
XLA Modules:
  0.0 64.0 jit_solution(12387611510268358540)
XLA Ops:
  0.0 63.3 %shard_map.82 = bf16[32,3072]{1,0:T(8,128)(2,1)S(1)} custom-call(bf16[32,3072]{1,0:T(8,128)(2,1)} %tok_ref.1, f32[1,3072]{1,0:T(1,128)} %bitcast.4, s32[4,32]{1,0:T(4,128)} %bitcast.5, f32[4,32]{1,0:T(4,128)} %bitcast.6, f32[1,32]{1,0:T(1,128)} %bitcast.7, bf16[1,3072,384]{2,1,0:T(8,128)(2,1)} %gate_hbm.1, bf16[1,3072,384]{2,1,0:T(8,128)(2,1)} %up_hbm.1, ...), custom_call_target="tpu_custom_call" | custom-call | tf_op jit(solution)/shard_map/pallas_call | solution.py:496
  63.3 0.7 %copy.10 = bf16[32,3072]{1,0:T(8,128)(2,1)} copy(bf16[32,3072]{1,0:T(8,128)(2,1)S(1)} %shard_map.82) | data formatting | bytes 393216

commit v5 on v4

--- a/solution.py
+++ b/solution.py
@@ -77,61 +77,63 @@
 
 
 END_ORDER = (
-    ("own", 0), ("own", 3), ("own", 2), ("firstq", 0, 0), ("own", 1), ("first", 3), ("line", 2, 1, 0),
-    ("line", 0, 1, 0), ("line", 3, 1, 0), ("firstq", 2, 1), ("line", 0, 2, 0), ("line", 0, 3, 0),
-    ("line", 1, 1, 1), ("last", 0, 0, 0), ("firstq", 0, 2), ("last", 0, 1, 0), ("firstq", 0, 1), ("first", 1),
-    ("last", 2, 1, 1), ("last", 0, 2, 0), ("firstq", 0, 3), ("last", 0, 3, 0), ("line", 3, 2, 0),
-    ("last", 3, 1, 0), ("line", 3, 1, 1), ("line", 3, 3, 1), ("last", 1, 1, 1), ("line", 3, 3, 0),
-    ("last", 0, 1, 1), ("last", 0, 2, 1), ("line", 3, 2, 1), ("last", 0, 0, 1), ("last", 0, 3, 1),
-    ("last", 2, 1, 0), ("last", 2, 0, 0), ("line", 1, 1, 0), ("last", 3, 0, 1), ("line", 2, 3, 0),
-    ("line", 2, 2, 0), ("firstq", 2, 0), ("hidden", 0), ("last", 3, 1, 1), ("line", 1, 2, 0),
-    ("last", 3, 2, 1), ("last", 3, 3, 0), ("last", 3, 0, 0), ("last", 1, 0, 1), ("last", 3, 3, 1),
-    ("last", 3, 2, 0), ("down", 0, 0), ("line", 1, 2, 1), ("line", 1, 3, 0), ("last", 2, 3, 0),
-    ("line", 1, 3, 1), ("firstq", 2, 2), ("last", 2, 2, 0), ("firstq", 2, 3), ("down", 0, 1),
-    ("last", 1, 1, 0), ("back", 0), ("last", 2, 0, 1), ("last", 1, 0, 0), ("hidden", 3), ("last", 1, 2, 1),
-    ("last", 1, 3, 0), ("last", 1, 2, 0), ("last", 1, 3, 1), ("down", 3, 0), ("hidden", 1), ("fsum", 0, 0),
-    ("down", 3, 1), ("back", 3), ("down", 1, 0), ("last", 2, 3, 1), ("last", 2, 2, 1), ("zsum", 0, 0),
-    ("down", 1, 1), ("back", 1), ("sum", 3, 0, 0), ("sum", 3, 0, 1), ("sum", 3, 1, 0), ("hidden", 2),
-    ("down", 2, 0), ("sum", 3, 2, 1), ("sum", 3, 1, 1), ("down", 2, 1), ("back", 2), ("sum", 1, 0, 1),
-    ("sum", 1, 0, 0), ("sum", 1, 1, 1), ("sum", 1, 2, 1), ("sum", 3, 2, 0), ("fsum", 2, 0), ("fsum", 2, 1),
-    ("sum", 1, 1, 0), ("fsum", 0, 1), ("zsum", 2, 0), ("fsum", 2, 3), ("zsum", 2, 1), ("home", 3, 1),
-    ("fsum", 2, 2), ("zsum", 0, 1), ("sum", 1, 2, 0), ("fsum", 0, 2), ("home", 1, 1), ("home", 3, 0),
-    ("zsum", 2, 2), ("final", 3), ("home", 1, 0), ("fsum", 0, 3), ("zsum", 0, 2), ("final", 1), ("homez", 0),
+    ("own", 0), ("own", 2), ("own", 1), ("line", 0, 1, 0), ("firstq", 0, 0), ("own", 3), ("first", 2),
+    ("line", 1, 1, 0), ("line", 0, 2, 0), ("first", 3), ("line", 1, 2, 0), ("firstq", 0, 2),
+    ("last", 3, 0, 0), ("last", 0, 0, 1), ("last", 0, 0, 0), ("firstq", 0, 1), ("line", 0, 3, 0),
+    ("last", 1, 0, 0), ("last", 3, 0, 1), ("last", 0, 2, 0), ("last", 2, 0, 1), ("line", 1, 3, 0),
+    ("last", 0, 1, 0), ("firstq", 0, 3), ("last", 1, 1, 0), ("firstq", 1, 1), ("last", 0, 1, 1),
+    ("firstq", 1, 2), ("line", 2, 1, 1), ("last", 0, 3, 0), ("firstq", 1, 3), ("firstq", 1, 0),
+    ("line", 2, 2, 1), ("last", 1, 3, 0), ("line", 2, 1, 0), ("last", 0, 2, 1), ("line", 2, 2, 0),
+    ("line", 3, 3, 0), ("last", 0, 3, 1), ("line", 3, 1, 0), ("hidden", 0), ("last", 1, 2, 0),
+    ("line", 2, 3, 0), ("line", 3, 2, 1), ("last", 1, 1, 1), ("last", 1, 3, 1), ("last", 1, 2, 1),
+    ("last", 1, 0, 1), ("line", 2, 3, 1), ("last", 2, 1, 1), ("down", 0, 0), ("last", 2, 1, 0),
+    ("down", 0, 1), ("line", 3, 3, 1), ("line", 3, 2, 0), ("line", 3, 1, 1), ("hidden", 1), ("last", 2, 2, 0),
+    ("back", 0), ("last", 2, 2, 1), ("last", 2, 3, 1), ("last", 2, 0, 0), ("last", 3, 2, 1),
+    ("last", 2, 3, 0), ("down", 1, 0), ("down", 1, 1), ("hidden", 2), ("last", 3, 1, 1), ("sum", 0, 0, 0),
+    ("last", 3, 3, 1), ("last", 3, 2, 0), ("back", 1), ("last", 3, 3, 0), ("last", 3, 1, 0), ("down", 2, 0),
+    ("down", 2, 1), ("sum", 0, 1, 0), ("hidden", 3), ("back", 2), ("sum", 0, 0, 1), ("sum", 0, 1, 1),
+    ("sum", 1, 0, 0), ("sum", 1, 1, 1), ("down", 3, 0), ("sum", 1, 0, 1), ("sum", 1, 1, 0), ("sum", 0, 2, 0),
+    ("sum", 1, 2, 1), ("sum", 0, 2, 1), ("down", 3, 1), ("back", 3), ("fsum", 3, 0), ("fsum", 2, 0),
+    ("sum", 1, 2, 0), ("fsum", 3, 1), ("fsum", 2, 1), ("zsum", 3, 0), ("fsum", 3, 2), ("zsum", 2, 0),
+    ("home", 1, 0), ("zsum", 2, 1), ("zsum", 3, 1), ("fsum", 2, 2), ("home", 1, 1), ("fsum", 3, 3),
+    ("zsum", 2, 2), ("home", 0, 0), ("zsum", 3, 2), ("final", 1), ("home", 0, 1), ("fsum", 2, 3),
+    ("homez", 3), ("homez", 2), ("drain_out", 0), ("drain_out", 1), ("drain_out", 2), ("drain_out", 3),
+    ("drain_back", 1), ("drain_back", 2), ("drain_back", 3), ("final", 0), ("drain_back", 0),
+)
+
+INNER_ORDER = (
+    ("own", 0), ("own", 2), ("own", 1), ("line", 0, 1, 0), ("line", 0, 2, 0), ("own", 3), ("line", 1, 2, 0),
+    ("line", 1, 1, 0), ("line", 2, 2, 0), ("line", 0, 3, 0), ("line", 2, 1, 0), ("line", 1, 3, 0),
+    ("line", 3, 2, 0), ("firstq", 0, 1), ("firstq", 0, 0), ("last", 1, 0, 0), ("firstq", 0, 2), ("first", 2),
+    ("first", 3), ("firstq", 0, 3), ("line", 2, 2, 1), ("line", 3, 3, 0), ("line", 3, 2, 1),
+    ("line", 2, 1, 1), ("last", 2, 2, 0), ("line", 3, 1, 1), ("line", 2, 3, 0), ("line", 2, 3, 1),
+    ("last", 0, 1, 0), ("last", 0, 0, 0), ("last", 0, 2, 0), ("firstq", 1, 0), ("last", 3, 2, 0),
+    ("last", 1, 1, 0), ("last", 2, 1, 0), ("line", 3, 1, 0), ("last", 0, 1, 1), ("last", 3, 0, 0),
+    ("last", 0, 3, 0), ("last", 0, 2, 1), ("line", 3, 3, 1), ("last", 0, 0, 1), ("last", 1, 3, 0),
+    ("last", 1, 2, 0), ("last", 0, 3, 1), ("hidden", 0), ("last", 3, 1, 1), ("last", 3, 2, 1),
+    ("last", 3, 0, 1), ("firstq", 1, 3), ("last", 3, 3, 0), ("firstq", 1, 2), ("firstq", 1, 1),
+    ("down", 0, 0), ("down", 0, 1), ("last", 1, 0, 1), ("last", 3, 3, 1), ("last", 3, 1, 0), ("back", 0),
+    ("last", 2, 0, 0), ("last", 2, 0, 1), ("last", 1, 3, 1), ("last", 1, 2, 1), ("hidden", 3),
+    ("last", 2, 1, 1), ("last", 1, 1, 1), ("last", 2, 2, 1), ("down", 3, 0), ("down", 3, 1), ("hidden", 1),
+    ("back", 3), ("down", 1, 0), ("down", 1, 1), ("last", 2, 3, 0), ("last", 2, 3, 1), ("sum", 0, 0, 0),
+    ("back", 1), ("hidden", 2), ("sum", 0, 0, 1), ("down", 2, 0), ("sum", 0, 2, 1), ("sum", 0, 2, 0),
+    ("sum", 1, 0, 0), ("fsum", 3, 3), ("fsum", 3, 1), ("down", 2, 1), ("back", 2), ("sum", 1, 0, 1),
+    ("sum", 1, 1, 0), ("fsum", 3, 0), ("fsum", 2, 0), ("sum", 1, 2, 0), ("sum", 1, 1, 1), ("fsum", 3, 2),
+    ("fsum", 2, 1), ("sum", 1, 2, 1), ("sum", 0, 1, 0), ("sum", 0, 1, 1), ("zsum", 3, 0), ("zsum", 2, 0),
+    ("fsum", 2, 2), ("home", 1, 1), ("zsum", 3, 2), ("zsum", 3, 1), ("fsum", 2, 3), ("home", 0, 1),
+    ("zsum", 2, 1), ("zsum", 2, 2), ("home", 1, 0), ("final", 1), ("homez", 3), ("home", 0, 0), ("final", 0),
     ("drain_out", 0), ("drain_out", 1), ("drain_out", 2), ("drain_out", 3), ("drain_back", 0),
     ("drain_back", 1), ("drain_back", 3), ("homez", 2), ("drain_back", 2),
 )
 
-INNER_ORDER = (
-    ("own", 0), ("own", 2), ("own", 1), ("own", 3), ("line", 0, 2, 0), ("line", 0, 1, 0), ("line", 2, 1, 0),
-    ("line", 3, 2, 0), ("first", 1), ("line", 0, 3, 0), ("firstq", 0, 0), ("firstq", 0, 2), ("line", 3, 3, 0),
-    ("firstq", 0, 1), ("line", 3, 2, 1), ("first", 3), ("firstq", 0, 3), ("line", 3, 1, 0), ("last", 0, 2, 0),
-    ("line", 3, 3, 1), ("line", 2, 2, 0), ("firstq", 2, 1), ("last", 2, 0, 0), ("line", 1, 2, 0),
-    ("line", 3, 1, 1), ("last", 0, 1, 0), ("line", 2, 3, 0), ("line", 1, 1, 0), ("line", 1, 1, 1),
-    ("last", 0, 2, 1), ("last", 0, 0, 0), ("last", 3, 0, 0), ("line", 1, 3, 0), ("last", 0, 0, 1),
-    ("line", 1, 2, 1), ("firstq", 2, 0), ("last", 3, 0, 1), ("last", 0, 3, 0), ("last", 3, 3, 0),
-    ("last", 0, 1, 1), ("last", 1, 0, 0), ("firstq", 2, 3), ("last", 3, 2, 1), ("last", 0, 3, 1),
-    ("last", 3, 1, 0), ("firstq", 2, 2), ("line", 1, 3, 1), ("hidden", 0), ("last", 1, 0, 1),
-    ("last", 3, 3, 1), ("down", 0, 0), ("down", 0, 1), ("last", 2, 1, 1), ("last", 3, 1, 1),
-    ("last", 3, 2, 0), ("back", 0), ("last", 2, 2, 0), ("last", 2, 3, 0), ("hidden", 3), ("last", 2, 0, 1),
-    ("last", 1, 2, 1), ("last", 2, 2, 1), ("last", 2, 3, 1), ("last", 2, 1, 0), ("down", 3, 0), ("hidden", 2),
-    ("last", 1, 1, 0), ("down", 3, 1), ("fsum", 0, 0), ("back", 3), ("last", 1, 1, 1), ("last", 1, 3, 1),
-    ("down", 2, 0), ("last", 1, 3, 0), ("down", 2, 1), ("last", 1, 2, 0), ("back", 2), ("hidden", 1),
-    ("down", 1, 0), ("sum", 3, 0, 0), ("down", 1, 1), ("sum", 3, 0, 1), ("back", 1), ("sum", 3, 2, 0),
-    ("sum", 3, 2, 1), ("sum", 1, 0, 0), ("sum", 3, 1, 0), ("fsum", 0, 2), ("fsum", 2, 0), ("sum", 1, 0, 1),
-    ("sum", 3, 1, 1), ("fsum", 2, 2), ("zsum", 0, 0), ("sum", 1, 1, 0), ("fsum", 2, 3), ("sum", 1, 2, 1),
-    ("sum", 1, 1, 1), ("fsum", 0, 1), ("fsum", 2, 1), ("zsum", 2, 0), ("fsum", 0, 3), ("sum", 1, 2, 0),
-    ("home", 3, 1), ("zsum", 0, 1), ("zsum", 2, 2), ("home", 1, 1), ("zsum", 0, 2), ("zsum", 2, 1),
-    ("home", 1, 0), ("final", 1), ("home", 3, 0), ("final", 3), ("homez", 0), ("drain_out", 0),
-    ("drain_out", 1), ("drain_out", 2), ("drain_out", 3), ("drain_back", 0), ("drain_back", 1),
-    ("drain_back", 3), ("homez", 2), ("drain_back", 2),
-)
-
-Z_FIRST_OUT = (True, False, True, False)
-Z_LAST_BACK = (True, False, True, False)
+LOADS_AT = 12
+Z_FIRST_OUT = (True, True, False, False)
+Z_LAST_BACK = (False, False, True, True)
 
 
 def ring_kernel(
-    zs, tok_ref, gain_ref, ids_ref, score_ref, prob_ref, gate_hbm, up_hbm, down_hbm, out_ref,
+    zs, tok_hbm, gain_hbm, ids_hbm, score_hbm, prob_hbm, gate_hbm, up_hbm, down_hbm, out_ref,
+    tok_ref, gain_ref, ids_ref, score_ref, prob_ref, in_sem,
     xg, stage, part, pair_in, last_in, line_in, first_in, fin_in, hid, scales, wgu, wd, w_sem,
     stage_send, stage_recv, gather_recv, own_send, first_send, line_send, last_send,
     mate_send, mate_recv, pair_send, pair_recv, back_send, back_recv, sum_send, sum_recv,
@@ -180,13 +182,15 @@
     blocks = 4 * zs
     inner = hid.shape[2]
 
-    copies = [
-        pltpu.make_async_copy(gate_hbm.at[0], wgu.at[:, : wgu.shape[1] // 2], w_sem.at[0]),
-        pltpu.make_async_copy(up_hbm.at[0], wgu.at[:, wgu.shape[1] // 2 :], w_sem.at[1]),
-        pltpu.make_async_copy(down_hbm.at[0, :, :half], wd.at[0], w_sem.at[2]),
-        pltpu.make_async_copy(down_hbm.at[0, :, half:], wd.at[1], w_sem.at[3]),
+    tok_copies = [
+        pltpu.make_async_copy(tok_hbm.at[pl.ds(j * rows, rows)], tok_ref.at[pl.ds(j * rows, rows)], in_sem.at[j])
+        for j in range(CHUNKS // 2)
     ]
-    for copy in copies:
+    small = [
+        pltpu.make_async_copy(src, dst, in_sem.at[2 + i])
+        for i, (src, dst) in enumerate(((gain_hbm, gain_ref), (ids_hbm, ids_ref), (score_hbm, score_ref), (prob_hbm, prob_ref)))
+    ]
+    for copy in (tok_copies[0], *small, tok_copies[1]):
         copy.start()
 
     barrier = pltpu.get_barrier_semaphore()
@@ -199,6 +203,12 @@
                 barrier, inc=1, device_id=(device(z - 1 + 2 * d, y, x, core),), device_id_type=MESH
             )
 
+    copies = [
+        pltpu.make_async_copy(gate_hbm.at[0], wgu.at[:, : wgu.shape[1] // 2], w_sem.at[0]),
+        pltpu.make_async_copy(up_hbm.at[0], wgu.at[:, wgu.shape[1] // 2 :], w_sem.at[1]),
+        pltpu.make_async_copy(down_hbm.at[0, :, :half], wd.at[0], w_sem.at[2]),
+        pltpu.make_async_copy(down_hbm.at[0, :, half:], wd.at[1], w_sem.at[3]),
+    ]
     def remote(src, dst, send_sem, recv_sem, target):
         return pltpu.make_async_remote_copy(
             src_ref=src, dst_ref=dst, send_sem=send_sem, recv_sem=recv_sem,
@@ -222,20 +232,44 @@
 
     own_slot = cols[0][0] + z
 
-    values = tok_ref[...].astype(jnp.float32)
-    average = jnp.sum(values, axis=1, keepdims=True) * (1.0 / model_width)
-    centred = values - average
-    variance = jnp.sum(centred * centred, axis=1, keepdims=True) * (1.0 / model_width)
-    normed = (centred * lax.rsqrt(variance + eps_norm) * gain_ref[...]).astype(jnp.bfloat16)
-    for c in (0, 1):
-        @pl.when(core == c)
-        def _():
-            for j in range(CHUNKS // 2):
-                piece = normed[j * rows : (j + 1) * rows]
+    def normalize(j):
+        values = tok_ref[j * rows : (j + 1) * rows].astype(jnp.float32)
+        average = jnp.sum(values, axis=1, keepdims=True) * (1.0 / model_width)
+        centred = values - average
+        variance = jnp.sum(centred * centred, axis=1, keepdims=True) * (1.0 / model_width)
+        piece = (centred * lax.rsqrt(variance + eps_norm) * gain_ref[...]).astype(jnp.bfloat16)
+        for c in (0, 1):
+            @pl.when(core == c)
+            def _():
                 mine = piece[:, :half] if c == 0 else piece[:, half:]
                 theirs = piece[:, half:] if c == 0 else piece[:, :half]
                 xg[c, 2 * j + c, own_slot, :, :half] = mine
                 stage[j] = theirs
+
+    def hand_over(j):
+        remote(stage.at[j], xg.at[other, 2 * j + core, own_slot, :, pl.ds(0, half)],
+               stage_send.at[j], stage_recv.at[2 * j + core], partner).start()
+
+    small[0].wait()
+    tok_copies[0].wait()
+    normalize(0)
+    inside = jnp.logical_and(has[0], has[1])
+
+    @pl.when(inside)
+    def _():
+        pl.semaphore_wait(barrier, 5)
+
+    @pl.when(jnp.logical_not(inside))
+    def _():
+        pl.semaphore_wait(barrier, 4)
+
+    hand_over(0)
+    for j in range(1, CHUNKS // 2):
+        tok_copies[j].wait()
+        normalize(j)
+        hand_over(j)
+    for copy in small[1:]:
+        copy.wait()
     score = [score_ref[k : k + 1, :] for k in range(TOP_K)]
     top = functools.reduce(jnp.maximum, score)
     exps = [jnp.exp(s - top) for s in score]
@@ -251,20 +285,6 @@
     tags = jnp.concatenate([tags, jnp.zeros((rows, LANES - count), jnp.float32)], axis=1)
     xg[core, 0, own_slot, :, half:] = tags.astype(jnp.bfloat16)
 
-    inside = jnp.logical_and(has[0], has[1])
-
-    @pl.when(inside)
-    def _():
-        pl.semaphore_wait(barrier, 5)
-
-    @pl.when(jnp.logical_not(inside))
-    def _():
-        pl.semaphore_wait(barrier, 4)
-
-    for j in range(CHUNKS // 2):
-        k = 2 * j + core
-        remote(stage.at[j], xg.at[core * 0 + other, k, own_slot, :, pl.ds(0, half)],
-               stage_send.at[j], stage_recv.at[k], partner).start()
 
     onward = jnp.where(z == 0, 1, z - 1)
 
@@ -448,7 +468,10 @@
         steps = dict(own=own, first=first, line=line, firstq=firstq, last=last, hidden=hidden, down=down,
                      back=back, sum=line_sum, zsum=zsum, fsum=fsum, home=home, homez=homez, final=final,
                      drain_out=drain_out, drain_back=drain_back)
-        for name, *rest in order:
+        for n, (name, *rest) in enumerate(order):
+            if n == LOADS_AT:
+                for copy in copies:
+                    copy.start()
             steps[name](*rest)
 
     pl.when(inside)(lambda: program(False, INNER_ORDER))
@@ -475,6 +498,9 @@
     dma = pltpu.SemaphoreType.DMA
     c = CHUNKS
     scratch = [
+        pltpu.VMEM((count, width), kind), pltpu.VMEM((1, width), jnp.float32),
+        pltpu.VMEM((TOP_K, count), jnp.int32), pltpu.VMEM((TOP_K, count), jnp.float32),
+        pltpu.VMEM((1, count), jnp.float32), dma((6,)),
         pltpu.VMEM((2, c, blocks, rows, half + LANES), kind),
         pltpu.VMEM((c // 2, rows, half), kind),
         pltpu.VMEM((2, c, blocks, rows, half), kind),
@@ -496,7 +522,7 @@
     return pl.pallas_call(
         functools.partial(ring_kernel, zs),
         out_shape=pltpu.VMEM((count, width), kind),
-        in_specs=[vmem] * 5 + [hbm] * 3,
+        in_specs=[hbm] * 8,
         out_specs=vmem,
         scratch_shapes=scratch,
         compiler_params=pltpu.CompilerParams(

time: 64.2 us -> 63.1 us (0.983)
  Pallas kernels: 63.3 us -> 62.2 us
    pallas_call x1, Pallas kernels: 63.3 us -> 62.2 us  [ring_local(): pl.pallas_call(functools.partial(ring_kernel, zs), out_shape=pltpu.VMEM((...]
where the time goes in v5:
time: 63.1 us; the launch traced here: 62.9 us
  Pallas kernels  62.2 us (99%)
  local copies, waits for them, and re-layouts  0.68 us (1%)
    pallas_call x1, Pallas kernels, ring_local(): pl.pallas_call(functools.partial(ring_kernel, zs), out_shape=pltpu.VMEM((...  62.2 us

profile of v5, /device:TPU:0, one launch (start us, length us, event | category | flops | bytes accessed | tf_op | source)
XLA Modules:
  0.0 62.9 jit_solution(357169407782603682)
XLA Ops:
  0.0 62.2 %shard_map.82 = bf16[32,3072]{1,0:T(8,128)(2,1)S(1)} custom-call(bf16[32,3072]{1,0:T(8,128)(2,1)} %tok_hbm.1, f32[1,3072]{1,0:T(1,128)} %bitcast.4, s32[4,32]{1,0:T(4,128)} %bitcast.5, f32[4,32]{1,0:T(4,128)} %bitcast.6, f32[1,32]{1,0:T(1,128)} %bitcast.7, bf16[1,3072,384]{2,1,0:T(8,128)(2,1)} %gate_hbm.1, bf16[1,3072,384]{2,1,0:T(8,128)(2,1)} %up_hbm.1, ...), custom_call_target="tpu_custom_call" | custom-call | tf_op jit(solution)/shard_map/pallas_call | solution.py:522
  62.2 0.7 %copy.10 = bf16[32,3072]{1,0:T(8,128)(2,1)} copy(bf16[32,3072]{1,0:T(8,128)(2,1)S(1)} %shard_map.82) | data formatting | bytes 393216

commit v6 on v5

--- a/solution.py
+++ b/solution.py
@@ -135,7 +135,7 @@
     zs, tok_hbm, gain_hbm, ids_hbm, score_hbm, prob_hbm, gate_hbm, up_hbm, down_hbm, out_ref,
     tok_ref, gain_ref, ids_ref, score_ref, prob_ref, in_sem,
     xg, stage, part, pair_in, last_in, line_in, first_in, fin_in, hid, scales, wgu, wd, w_sem,
-    stage_send, stage_recv, gather_recv, own_send, first_send, line_send, last_send,
+    stage_send, stage_recv, gather_recv, first_send, line_send, last_send,
     mate_send, mate_recv, pair_send, pair_recv, back_send, back_recv, sum_send, sum_recv,
     home_send, home_recv, fin_send, fin_recv,
 ):
@@ -300,9 +300,9 @@
             ref = block(core, k, slot)
             sem = gather_recv.at[k, slot]
             if i == 0:
-                out_z(ref, k, slot, lambda n: own_send.at[k, n])
+                out_z(ref, k, slot, lambda n: line_send.at[k])
             elif not at_end:
-                remote(ref, ref, line_send.at[k, i], sem, device(away[i], y, x, core)).start()
+                remote(ref, ref, line_send.at[k], sem, device(away[i], y, x, core)).start()
             if Z_FIRST_OUT[k] and fr == 0:
                 remote(ref, ref, first_send.at[k], sem, first_dev).start()
             remote(ref, ref, last_send.at[k], sem, last_dev).start()
@@ -452,10 +452,7 @@
                 sent(stage.at[k // 2], stage_send.at[k // 2])
             wide_z = 1 if Z_FIRST_OUT[k] else 2
             sent(span(core, k, zs if Z_FIRST_OUT[k] else 1), first_send.at[k])
-            for n in (0,) if at_end else (0, 1):
-                sent(span(core, k, wide_z), own_send.at[k, n])
-            for i in () if at_end else range(1, zs):
-                sent(span(core, k, wide_z), line_send.at[k, i])
+            sent(span(core, k, wide_z * (1 if at_end else zs + 1)), line_send.at[k])
             sent(span(core, k, 2 * zs), last_send.at[k])
             sent(span(core, k, blocks), mate_send.at[k])
 
@@ -514,7 +511,7 @@
         pltpu.VMEM((width, 2 * inner), kind),
         pltpu.VMEM((2, inner, half), kind),
         dma((4,)),
-        dma((c // 2,)), dma((c,)), dma((c, blocks)), dma((c, 2)), dma((c,)), dma((c, zs)), dma((c,)),
+        dma((c // 2,)), dma((c,)), dma((c, blocks)), dma((c,)), dma((c,)), dma((c,)),
         dma((c,)), dma((c,)), dma((c,)), dma((c,)), dma((c,)), dma((c, 2, zs)),
         dma((c,)), dma((c, 2, 2, zs)),
         dma((c,)), dma((c, zs)), dma((c // 2,)), dma((c // 2,)),

time: 63.1 us -> 62.9 us (level)
  no operation moved by 1% of the time
where the time goes in v6:
time: 62.9 us; the launch traced here: 62.7 us
  Pallas kernels  62.1 us (99%)
  local copies, waits for them, and re-layouts  0.68 us (1%)
    pallas_call x1, Pallas kernels, ring_local(): pl.pallas_call(functools.partial(ring_kernel, zs), out_shape=pltpu.VMEM((...  62.1 us

profile of v6, /device:TPU:0, one launch (start us, length us, event | category | flops | bytes accessed | tf_op | source)
XLA Modules:
  0.0 62.7 jit_solution(10770204887468249923)
XLA Ops:
  0.0 62.1 %shard_map.82 = bf16[32,3072]{1,0:T(8,128)(2,1)S(1)} custom-call(bf16[32,3072]{1,0:T(8,128)(2,1)} %tok_hbm.1, f32[1,3072]{1,0:T(1,128)} %bitcast.4, s32[4,32]{1,0:T(4,128)} %bitcast.5, f32[4,32]{1,0:T(4,128)} %bitcast.6, f32[1,32]{1,0:T(1,128)} %bitcast.7, bf16[1,3072,384]{2,1,0:T(8,128)(2,1)} %gate_hbm.1, bf16[1,3072,384]{2,1,0:T(8,128)(2,1)} %up_hbm.1, ...), custom_call_target="tpu_custom_call" | custom-call | tf_op jit(solution)/shard_map/pallas_call | solution.py:519
  62.1 0.7 %copy.10 = bf16[32,3072]{1,0:T(8,128)(2,1)} copy(bf16[32,3072]{1,0:T(8,128)(2,1)S(1)} %shard_map.82) | data formatting | bytes 393216
